TPU v7x, 32 devices: a whole 2x2x4 slice. The times are simulated.
32 devices in a mesh: rep: 2 (over x), fs: 8 (over z, y), tp: 2 (over core).
Axes of the slice: x: 2, y: 2, z: 4, core: 2. Of those that a mesh axis runs over, the one named last changes fastest.
Arguments:
- incoming_features: bfloat16 [3072, 2048], P(('rep', 'fs'), 'tp'), may hold values from -6 to 6
- attend_prenormal_scale: bfloat16 [2048], replicated, may hold values from 0.099609375 to 1.8984375
- probe_matrix: bfloat16 [2048, 512], P('fs', 'tp'), may hold values from -0.125 to 0.125
- lookup_matrix: bfloat16 [2048, 512], P('fs', 'tp'), may hold values from -0.125 to 0.125
- content_matrix: bfloat16 [2048, 1024], P('fs', 'tp'), may hold values from -0.125 to 0.125
- forgetting_matrix: bfloat16 [2048, 512], P('fs', 'tp'), may hold values from -0.125 to 0.125
- result_switch_matrix: bfloat16 [2048, 1024], P('fs', 'tp'), may hold values from -0.125 to 0.125
- forgetting_shift: float32 [512], P('tp'), may hold values from -0.5 to 5.5
- spike_forget_logarithm: float32 [3072, 512], P(('rep', 'fs'), 'tp'), may hold values from -0.7 to 0
- attend_unit_scale: bfloat16 [1024], P('tp'), may hold values from 0.099609375 to 1.8984375
- attend_result_matrix: bfloat16 [1024, 2048], P('tp', 'fs'), may hold values from -0.1875 to 0.1875
- perceptron_scale: bfloat16 [2048], replicated, may hold values from 0.099609375 to 1.8984375
- content_expand_matrix: bfloat16 [2048, 4096], P('fs', 'tp'), may hold values from -0.125 to 0.125
- switch_expand_matrix: bfloat16 [2048, 4096], P('fs', 'tp'), may hold values from -0.125 to 0.125
- content_kernel: bfloat16 [3, 4096], P(None, 'tp'), may hold values from -3.5 to 3.5
- switch_kernel: bfloat16 [3, 4096], P(None, 'tp'), may hold values from -3.5 to 3.5
- contract_matrix: bfloat16 [4096, 2048], P('tp', 'fs'), may hold values from -0.09375 to 0.09375
Outputs:
- out_rows: bfloat16 [3072, 2048], P(('rep', 'fs'), 'tp')
All inputs are finite; a program needn't handle non-finite values.
Results may differ from a plain program's by a relative error of at most 0.02.
Values may be sent and summed in bfloat16 or wider, within the bound.
No kernel may reach another device: no remote copies, remote signals or barrier semaphores. Data moves between devices by JAX's collectives and lax.ppermute only.
A program may use at most 64 MiB of HBM per device.

v0:
```python
import jax
import jax.numpy as jnp
from jax import lax
from jax.experimental import pallas as pl
from jax.experimental.pallas import tpu as pltpu
from jax.sharding import Mesh
from jax.sharding import PartitionSpec as P


HEAD_K = 32
HEAD_V = 64
BLOCK = 64
SUB = 8
LANES = 128

norm_eps = 1e-06
switch_multiplier = 16.0


def row_norm(content_tokens, gain):
    content_tokens = content_tokens.astype(jnp.float32)
    scaled = content_tokens * lax.rsqrt(
        jnp.mean(content_tokens * content_tokens, axis=-1, keepdims=True) + norm_eps
    )
    return (scaled * gain.astype(jnp.float32)).astype(jnp.bfloat16)


def gated_scan(probe_tokens, lookup_tokens, content_tokens, forgetting_scores):
    length, heads, key_size = probe_tokens.shape
    value_size = content_tokens.shape[-1]
    blocks = length // BLOCK

    def split_blocks(array):
        return array.reshape(blocks, BLOCK, heads, array.shape[-1])

    causal = jnp.arange(BLOCK)[:, None] >= jnp.arange(BLOCK)[None, :]
    highest = lax.Precision.HIGHEST

    def step(state, incoming_tokens):
        query_block, key_block, value_block, decay_block = incoming_tokens
        cumulative = jnp.cumsum(decay_block, axis=0)
        differ = cumulative[:, None] - cumulative[None, :]
        weight = jnp.exp(jnp.where(causal[:, :, None, None], differ, -jnp.inf))
        scores = jnp.einsum("thd,shd,tshd->tsh", query_block, key_block, weight, precision=highest)
        inner = jnp.einsum("tsh,shv->thv", scores, value_block, precision=highest)
        carried = jnp.einsum(
            "thd,hdv->thv", query_block * jnp.exp(cumulative), state, precision=highest
        )
        final = cumulative[-1]
        state = jnp.exp(final)[:, :, None] * state + jnp.einsum(
            "shd,shv->hdv",
            key_block * jnp.exp(final[None] - cumulative),
            value_block,
            precision=highest,
        )
        return (state, inner + carried)

    start_state = jnp.zeros((heads, key_size, value_size), jnp.float32)
    _, result_tokens = lax.scan(
        step,
        start_state,
        (
            split_blocks(probe_tokens),
            split_blocks(lookup_tokens),
            split_blocks(content_tokens),
            split_blocks(forgetting_scores),
        ),
    )
    return result_tokens.reshape(length, heads, value_size)


def attend_unit_results(
    probe_tokens,
    lookup_tokens,
    content_tokens,
    result_switch,
    forgetting_raw,
    spike_forgetting,
    attend_unit_scale,
):
    length = probe_tokens.shape[0]
    heads = probe_tokens.shape[1] // HEAD_K
    forgetting_scores = jax.nn.log_sigmoid(forgetting_raw) / switch_multiplier + spike_forgetting

    def split_heads(array, width):
        return array.astype(jnp.float32).reshape(length, heads, width)

    result_tokens = gated_scan(
        split_heads(probe_tokens, HEAD_K) * HEAD_K ** (-0.5),
        split_heads(lookup_tokens, HEAD_K),
        split_heads(content_tokens, HEAD_V),
        split_heads(forgetting_scores, HEAD_K),
    )
    result_tokens = result_tokens * lax.rsqrt(
        jnp.mean(result_tokens * result_tokens, axis=-1, keepdims=True) + norm_eps
    )
    result_tokens = result_tokens * attend_unit_scale.astype(jnp.float32).reshape(heads, HEAD_V)
    switched_result = result_tokens.reshape(length, heads * HEAD_V) * jax.nn.silu(
        result_switch.astype(jnp.float32)
    )
    return switched_result.astype(jnp.bfloat16)


def causal_conv(content_tokens, taps):
    content_tokens = content_tokens.astype(jnp.float32)
    taps = taps.astype(jnp.float32)
    width = taps.shape[0]
    padded = jnp.pad(content_tokens, ((width - 1, 0), (0, 0)))
    total = jnp.zeros_like(content_tokens)
    for offset in range(width):
        total = total + padded[offset : offset + content_tokens.shape[0]] * taps[offset]
    return total


def general_shards(
    incoming_features,
    attend_prenormal_scale,
    probe_matrix,
    lookup_matrix,
    content_matrix,
    forgetting_matrix,
    result_switch_matrix,
    forgetting_shift,
    spike_forget_logarithm,
    attend_unit_scale,
    attend_result_matrix,
    perceptron_scale,
    content_expand_matrix,
    switch_expand_matrix,
    content_kernel,
    switch_kernel,
    contract_matrix,
):
    whole_in = lax.all_gather(incoming_features, "tp", axis=1, tiled=True)
    columns = row_norm(whole_in, attend_prenormal_scale)
    pieces = tuple(
        lax.all_gather(piece, "fs", axis=0, tiled=True)
        for piece in (
            probe_matrix,
            lookup_matrix,
            content_matrix,
            forgetting_matrix,
            result_switch_matrix,
        )
    )
    query_sum, key_sum, value_sum, decay_sum, gate_sum = tuple(
        (jnp.dot(columns, piece, preferred_element_type=jnp.float32) for piece in pieces)
    )
    switched_result = attend_unit_results(
        query_sum.astype(jnp.bfloat16),
        key_sum.astype(jnp.bfloat16),
        value_sum.astype(jnp.bfloat16),
        gate_sum.astype(jnp.bfloat16),
        decay_sum + forgetting_shift,
        spike_forget_logarithm,
        attend_unit_scale,
    )
    mixer_partial = jnp.dot(
        switched_result,
        lax.all_gather(attend_result_matrix, "fs", axis=1, tiled=True),
        preferred_element_type=jnp.float32,
    )
    mix = lax.psum_scatter(
        mixer_partial.astype(jnp.bfloat16), "tp", scatter_dimension=1, tiled=True
    )
    middle = (
        incoming_features.astype(jnp.float32) + lax.optimization_barrier(mix).astype(jnp.float32)
    ).astype(jnp.bfloat16)
    whole_mid = lax.all_gather(middle, "tp", axis=1, tiled=True)
    columns = row_norm(whole_mid, perceptron_scale)
    pieces = (
        lax.all_gather(content_expand_matrix, "fs", axis=0, tiled=True),
        lax.all_gather(switch_expand_matrix, "fs", axis=0, tiled=True),
    )
    value_total = jnp.dot(columns, pieces[0], preferred_element_type=jnp.float32)
    gate_total = jnp.dot(columns, pieces[1], preferred_element_type=jnp.float32)
    conv_value = causal_conv(value_total.astype(jnp.bfloat16), content_kernel)
    conv_gated = causal_conv(gate_total.astype(jnp.bfloat16), switch_kernel)
    hidden = (conv_value * jax.nn.gelu(conv_gated, approximate=True)).astype(jnp.bfloat16)
    down_partial = jnp.dot(
        hidden,
        lax.all_gather(contract_matrix, "fs", axis=1, tiled=True),
        preferred_element_type=jnp.float32,
    )
    ffn = lax.psum_scatter(down_partial.astype(jnp.bfloat16), "tp", scatter_dimension=1, tiled=True)
    return (middle.astype(jnp.float32) + lax.optimization_barrier(ffn).astype(jnp.float32)).astype(
        jnp.bfloat16
    )


F32 = jnp.float32
BF16 = jnp.bfloat16


def dot(a, b):
    return jnp.dot(a, b, preferred_element_type=F32)


def pack_kernel(pos, probe, lookup, content, forget, switch, result, own, send):
    quarter, across = pos[0], pos[1]
    rows = probe.shape[0]
    half = rows // 2
    key_w = probe.shape[1] // 4
    val_w = content.shape[1] // 4
    part = result.shape[0] // 4

    def pack(index, out):
        for q in range(4):

            @pl.when(index == q)
            def _():
                keys = pl.ds(q * key_w, key_w)
                vals = pl.ds(q * val_w, val_w)
                out[0:rows, :] = jnp.concatenate([probe[:, keys], lookup[:, keys]], axis=1)
                out[rows : 2 * rows, :] = content[:, vals]
                out[2 * rows : 3 * rows, :] = switch[:, vals]
                base = 3 * rows
                out[base : base + part, :] = result[q * part : (q + 1) * part, 0:LANES]
                out[base + part : base + 2 * part, :] = result[q * part : (q + 1) * part, LANES:]
                base = base + 2 * part
                decay = forget[:, keys]
                out[base : base + half, :] = jnp.concatenate(
                    [decay[:half], decay[half:]], axis=1
                )

    pack(across, send)
    pack(quarter, own)


def input_kernel(pos, spike, feat, own_spike, to_x, to_y, to_d):
    key_w = spike.shape[1] // 4
    width = feat.shape[1]

    def spikes(index):
        value = spike[:, 0:key_w]
        for q in range(1, 4):
            value = jnp.where(index == q, spike[:, q * key_w : (q + 1) * key_w], value)
        high = value.astype(BF16)
        low = (value - high.astype(F32)).astype(BF16)
        return jnp.concatenate([high, low], axis=1)

    own_spike[...] = spikes(pos[0])
    for slot, ref in ((2, to_x), (3, to_y), (4, to_d)):
        ref[:, 0:width] = feat[...]
        ref[:, width:] = spikes(pos[slot])


def copy_from(choices, sem, dst, cut):
    for cond, ref in choices:
        copy = pltpu.make_async_copy(cut(ref), dst, sem)
        if cond is None:
            copy.start()
        else:
            pl.when(cond)(copy.start)


def blocks_of(pos, slots):
    slot_o, slot_r1, slot_l1, slot_r2, slot_l2, slot_r3, slot_l3 = slots
    z, last = pos[6], pos[8]
    low = z < 2
    first_z = z == 0
    last_z = z == last
    return (
        (z, ((None, slot_o),)),
        (jnp.bitwise_xor(z, 2), ((low, slot_l2), (jnp.logical_not(low), slot_r2))),
        (
            jnp.where(first_z, last, z - 1),
            ((first_z, slot_l3), (jnp.logical_not(first_z), slot_r1)),
        ),
        (
            jnp.where(last_z, 0, z + 1),
            ((last_z, slot_r3), (jnp.logical_not(last_z), slot_l1)),
        ),
    )


def attend_kernel(
    pos, mine, theirs, scale, shift, unit, spike_o, spike_x, spike_y, spike_d,
    slot_o, slot_r1, slot_l1, slot_r2, slot_l2, slot_r3, slot_l3,
    keep, send,
    w_qk, w_vg, w_f, w_o, folded, qk_s, v_s, g_s, f_s, gated, sems,
):
    core, y = pos[5], pos[7]
    rows = slot_o.shape[0] // 2
    chunk = w_qk.shape[0] // 8
    half = chunk // 2
    part = w_o.shape[1]
    span = spike_o.shape[0]
    length, width = mine.shape
    key_w = f_s.shape[1] // 2

    slots = (slot_o, slot_r1, slot_l1, slot_r2, slot_l2, slot_r3, slot_l3)
    waits = []
    for index, (zi, choices) in enumerate(blocks_of(pos, slots)):
        for j in range(2):
            shard = zi * 2 + (y if j == 0 else 1 - y)
            at = pl.ds(pl.multiple_of(shard * chunk, chunk), chunk)
            base = j * rows
            targets = (
                (w_qk.at[at, :], chunk),
                (w_vg.at[at, 0:LANES], chunk),
                (w_vg.at[at, LANES : 2 * LANES], chunk),
                (w_o.at[shard, :, 0:LANES], part),
                (w_o.at[shard, :, LANES : 2 * LANES], part),
                (folded.at[shard], half),
            )
            for k, (dst, size) in enumerate(targets):
                sem = sems.at[index * 12 + j * 6 + k]
                copy_from(choices, sem, dst, lambda ref, b=base, n=size: ref.at[pl.ds(b, n), :])
                waits.append((slot_o.at[pl.ds(base, size), :], dst, sem))
                base += size
    for source, dst, sem in waits:
        pltpu.make_async_copy(source, dst, sem).wait()
    for shard in range(8):
        w_f[shard * chunk : shard * chunk + half, :] = folded[shard]
        w_f[shard * chunk + half : (shard + 1) * chunk, :] = pltpu.roll(
            folded[shard].astype(F32), key_w, 1
        ).astype(BF16)

    def project(s, carry):
        at = pl.ds(pl.multiple_of(s * span, span), span)
        a = mine[at, :].astype(F32)
        b = theirs[at, :].astype(F32)
        total = jnp.sum(a * a, axis=1, keepdims=True) + jnp.sum(b * b, axis=1, keepdims=True)
        inverse = lax.rsqrt(total / scale.shape[1] + norm_eps)
        low = jnp.where(core == 0, a, b)
        high = jnp.where(core == 0, b, a)
        width = a.shape[1]
        normed = jnp.concatenate(
            [
                (low * inverse * scale[:, 0:width].astype(F32)).astype(BF16),
                (high * inverse * scale[:, width:].astype(F32)).astype(BF16),
            ],
            axis=1,
        )
        qk_s[at, :] = dot(normed, w_qk[...]).astype(BF16).astype(F32)
        vg = dot(normed, w_vg[...]).astype(BF16)
        v_s[at, :] = vg[:, 0:LANES]
        g_s[at, :] = vg[:, LANES:]
        f_s[at, :] = dot(normed, w_f[...])
        return carry

    count = length // span
    lax.fori_loop(0, count, project, 0)

    lane = lax.broadcasted_iota(jnp.int32, (span, LANES), 1)
    left = lane < key_w
    row = lax.broadcasted_iota(jnp.int32, (span, LANES), 0)
    lane_head = lax.broadcasted_iota(jnp.int32, (LANES, 2 * LANES), 0) // HEAD_K
    wide_head = lax.broadcasted_iota(jnp.int32, (LANES, 2 * LANES), 1) // HEAD_V
    spread = (lane_head == wide_head).astype(BF16)
    wide_a = lax.broadcasted_iota(jnp.int32, (2 * LANES, 2 * LANES), 0) // HEAD_V
    wide_b = lax.broadcasted_iota(jnp.int32, (2 * LANES, 2 * LANES), 1) // HEAD_V
    same_wide = (wide_a == wide_b).astype(BF16)
    tri = (
        lax.broadcasted_iota(jnp.int32, (span, span), 0)
        >= lax.broadcasted_iota(jnp.int32, (span, span), 1)
    ).astype(BF16)
    heads = LANES // HEAD_K

    def split_dot(a, value):
        one = value.astype(BF16)
        rest = value - one.astype(F32)
        two = rest.astype(BF16)
        three = (rest - two.astype(F32)).astype(BF16)
        return dot(a, one) + dot(a, two) + dot(a, three)

    def pair(p, carry):
        at_a = pl.ds(pl.multiple_of(p * 2 * span, span), span)
        at_b = pl.ds(pl.multiple_of(p * 2 * span + span, span), span)
        qk_a, qk_b = qk_s[at_a, :], qk_s[at_b, :]
        query = jnp.where(left, qk_a, pltpu.roll(qk_b, key_w, 1)) * HEAD_K ** (-0.5)
        keys = jnp.where(left, pltpu.roll(qk_a, key_w, 1), qk_b)
        v_a, v_b = v_s[at_a, :], v_s[at_b, :]
        value = jnp.concatenate([v_a, v_b], axis=1)
        decay = jnp.where(left, f_s[at_a, :], pltpu.roll(f_s[at_b, :], key_w, 1))
        decay = decay + shift[...]
        spike_a = jnp.where(p == 0, spike_o[...], spike_y[:, width:]).astype(F32)
        spike_b = jnp.where(p == 0, spike_x[:, width:], spike_d[:, width:]).astype(F32)
        spike_a = spike_a + pltpu.roll(spike_a, key_w, 1)
        spike_b = spike_b + pltpu.roll(spike_b, key_w, 1)
        soft = jnp.minimum(decay, 0.0) - jnp.log1p(jnp.exp(-jnp.abs(decay)))
        log_decay = soft / switch_multiplier + jnp.where(left, spike_a, spike_b)
        cum = split_dot(tri, log_decay)

        tiles = span // SUB
        q3 = query.reshape(tiles, SUB, LANES)
        k3 = keys.reshape(tiles, SUB, LANES)
        c3 = cum.reshape(tiles, SUB, LANES)
        valuef = value.astype(F32)
        v3 = valuef.reshape(tiles, SUB, 2 * LANES)
        place = lax.broadcasted_iota(jnp.int32, (tiles, SUB, LANES), 1)
        out = jnp.zeros((span, 2 * LANES), F32)
        for lag in range(SUB):
            if lag == 0:
                term = q3 * k3
                v_lag = v3
            else:
                k_lag = pltpu.roll(k3, lag, 1)
                c_lag = pltpu.roll(c3, lag, 1)
                v_lag = pltpu.roll(v3, lag, 1)
                fall = jnp.exp(jnp.where(place >= lag, c3 - c_lag, -jnp.inf))
                term = q3 * k_lag * fall
            spread_term = dot(term.reshape(span, LANES).astype(BF16), spread)
            out = out + spread_term * v_lag.reshape(span, 2 * LANES)

        size = SUB
        while size < span:
            blocks = max(span // (2 * size), 1)
            if 2 * size > span:
                second_rows = span - size
            else:
                second_rows = size
            begin = [i * 2 * size for i in range(blocks)]
            q_parts, k_parts, v_parts = [], [], []
            for b0 in begin:
                middle = b0 + size
                ref_row = cum[middle - 1 : middle, :]
                q_parts.append(
                    query[middle : middle + second_rows]
                    * jnp.exp(cum[middle : middle + second_rows] - ref_row)
                )
                k_parts.append(keys[b0:middle] * jnp.exp(ref_row - cum[b0:middle]))
                v_parts.append(value[b0:middle] if size % 16 == 0 else valuef[b0:middle])
            q_all = jnp.concatenate(q_parts, axis=0) if blocks > 1 else q_parts[0]
            k_all = jnp.concatenate(k_parts, axis=0) if blocks > 1 else k_parts[0]
            v_all = (jnp.concatenate(v_parts, axis=0) if blocks > 1 else v_parts[0]).astype(BF16)
            n_q, n_k = q_all.shape[0], k_all.shape[0]
            q_lane = lax.broadcasted_iota(jnp.int32, (n_q, LANES), 1) // HEAD_K
            q_heads = jnp.concatenate(
                [jnp.where(q_lane == h, q_all, 0.0) for h in range(heads)], axis=0
            ).astype(BF16)
            scores = lax.dot_general(
                q_heads, k_all.astype(BF16), (((1,), (1,)), ((), ())), preferred_element_type=F32
            )
            if blocks > 1:
                q_block = (
                    lax.rem(lax.broadcasted_iota(jnp.int32, (heads * n_q, n_k), 0), n_q)
                    // second_rows
                )
                k_block = lax.broadcasted_iota(jnp.int32, (heads * n_q, n_k), 1) // size
                scores = jnp.where(q_block == k_block, scores, 0.0)
            wide = dot(scores.astype(BF16), v_all)
            wide_lane = lax.broadcasted_iota(jnp.int32, (n_q, 2 * LANES), 1) // HEAD_V
            total = wide[0:n_q]
            for h in range(1, heads):
                total = jnp.where(wide_lane == h, wide[h * n_q : (h + 1) * n_q], total)
            zeros = jnp.zeros((size, 2 * LANES), F32)
            full = []
            for i in range(blocks):
                full.append(zeros)
                full.append(total[i * second_rows : (i + 1) * second_rows])
            covered = blocks * size + blocks * second_rows
            if covered < span:
                full.append(jnp.zeros((span - covered, 2 * LANES), F32))
            out = out + jnp.concatenate(full, axis=0)
            size *= 2

        square = out * out
        high = square.astype(BF16)
        low = (square - high.astype(F32)).astype(BF16)
        mean = (dot(high, same_wide) + dot(low, same_wide)) / HEAD_V
        out = out * lax.rsqrt(mean + norm_eps)
        gate = jnp.concatenate([g_s[at_a, :], g_s[at_b, :]], axis=1).astype(F32)
        gain = unit[...].astype(F32)
        out = out * jnp.concatenate([gain, gain], axis=1)
        out = out * (gate / (1.0 + jnp.exp(-gate)))
        gated[at_a, :] = out[:, 0:LANES].astype(BF16)
        gated[at_b, :] = out[:, LANES:].astype(BF16)
        return carry

    lax.fori_loop(0, count // 2, pair, 0)
    mix_out(core, gated, w_o, keep, send)


def mix_out(core, left, weights, keep, send):
    shards = weights.shape[0]
    width = weights.shape[2]
    for h in range(2):
        for f in range(shards // 2):
            w = weights[h * (shards // 2) + f]
            value = dot(left[...], w).astype(BF16)
            cols = slice(f * width, (f + 1) * width)

            @pl.when(core == h)
            def _():
                keep[:, cols] = value

            @pl.when(core != h)
            def _():
                send[:, cols] = value


def expand_kernel(
    pos, mine, theirs, scale, taps_v, taps_g,
    slot_o, slot_r1, slot_l1, slot_r2, slot_l2, slot_r3, slot_l3,
    hidden, w_up, sems,
):
    core, y = pos[5], pos[7]
    chunk = slot_o.shape[0] // 2
    span = hidden.shape[0] // 4
    width = hidden.shape[1]

    slots = (slot_o, slot_r1, slot_l1, slot_r2, slot_l2, slot_r3, slot_l3)
    waits = []
    for index, (zi, choices) in enumerate(blocks_of(pos, slots)):
        for j in range(2):
            side = y if j == 0 else 1 - y
            dst = w_up.at[pl.ds(pl.multiple_of((zi * 2 + side) * chunk, chunk), chunk), :]
            sem = sems.at[index * 2 + j]
            copy_from(choices, sem, dst, lambda ref, b=j * chunk: ref.at[pl.ds(b, chunk), :])
            waits.append((slot_o.at[pl.ds(j * chunk, chunk), :], dst, sem))
    for source, dst, sem in waits:
        pltpu.make_async_copy(source, dst, sem).wait()

    def conv(value, taps):
        taps = taps.astype(F32)
        row = lax.broadcasted_iota(jnp.int32, value.shape, 0)
        total = value * taps[2:3]
        total = total + jnp.where(row >= 1, pltpu.roll(value, 1, 0), 0.0) * taps[1:2]
        return total + jnp.where(row >= 2, pltpu.roll(value, 2, 0), 0.0) * taps[0:1]

    def sequence(s, carry):
        at = pl.ds(pl.multiple_of(s * span, span), span)
        a = mine[at, :].astype(F32)
        b = theirs[at, :].astype(F32)
        total = jnp.sum(a * a, axis=1, keepdims=True) + jnp.sum(b * b, axis=1, keepdims=True)
        inverse = lax.rsqrt(total / scale.shape[1] + norm_eps)
        low = jnp.where(core == 0, a, b)
        high = jnp.where(core == 0, b, a)
        half = a.shape[1]
        normed = jnp.concatenate(
            [
                (low * inverse * scale[:, 0:half].astype(F32)).astype(BF16),
                (high * inverse * scale[:, half:].astype(F32)).astype(BF16),
            ],
            axis=1,
        )
        value = dot(normed, w_up[:, 0:width]).astype(BF16).astype(F32)
        gate = dot(normed, w_up[:, width:]).astype(BF16).astype(F32)
        value = conv(value, taps_v[...])
        gate = conv(gate, taps_g[...])
        hidden[at, :] = (value * jax.nn.gelu(gate, approximate=True)).astype(BF16)
        return carry

    lax.fori_loop(0, 4, sequence, 0)


def contract_pair(pos, hidden, blocks, keep, send, weights, sems):
    y = pos[7]
    rows = weights.shape[2]
    width = weights.shape[3]
    waits = []
    for index, (where, choices) in enumerate(blocks):
        for j in range(2):
            dst = weights.at[where, y if j == 0 else 1 - y]
            sem = sems.at[index * 2 + j]
            copy_from(choices, sem, dst, lambda ref, b=j * rows: ref.at[pl.ds(b, rows), :])
            waits.append((choices[0][1].at[pl.ds(j * rows, rows), :], dst, sem))
    for source, dst, sem in waits:
        pltpu.make_async_copy(source, dst, sem).wait()
    for index, out in ((1, send), (0, keep)):
        for side in range(2):
            out[:, side * width : (side + 1) * width] = dot(
                hidden[...], weights[index, side]
            ).astype(BF16)


def contract_kernel_one(pos, hidden, slot_o, slot_r2, slot_l2, keep, send, weights, sems):
    z = pos[6]
    same = jnp.where((z // 2) == pos[5], 0, 1)
    low = z < 2
    blocks = (
        (same, ((None, slot_o),)),
        (1 - same, ((low, slot_l2), (jnp.logical_not(low), slot_r2))),
    )
    contract_pair(pos, hidden, blocks, keep, send, weights, sems)


def contract_kernel_two(
    pos, hidden, slot_r1, slot_l1, slot_r3, slot_l3, keep, send, weights, sems
):
    z, last = pos[6], pos[8]
    same = jnp.where((z // 2) == pos[5], 0, 1)
    even = lax.rem(z, 2) == 0
    blocks = (
        (same, ((even, slot_l1), (jnp.logical_not(even), slot_r1))),
        (
            1 - same,
            ((z == 0, slot_l3), (z == 1, slot_l1), (z == 2, slot_r1), (z == last, slot_r3)),
        ),
    )
    contract_pair(pos, hidden, blocks, keep, send, weights, sems)


def call(kernel, outs, args, scratch=(), flops=0, free=0):
    in_specs = [pl.BlockSpec(memory_space=pltpu.SMEM)]
    in_specs += [pl.BlockSpec(memory_space=pltpu.VMEM)] * (len(args) - 1 - free)
    in_specs += [pl.BlockSpec(memory_space=pl.ANY)] * free
    return pl.pallas_call(
        kernel,
        out_shape=[jax.ShapeDtypeStruct(*o) for o in outs],
        in_specs=in_specs,
        out_specs=[pl.BlockSpec(memory_space=pltpu.VMEM)] * len(outs),
        scratch_shapes=list(scratch),
        cost_estimate=pl.CostEstimate(flops=flops, bytes_accessed=1 << 20, transcendentals=0),
        compiler_params=pltpu.CompilerParams(vmem_limit_bytes=56 << 20),
    )(*args)


def plane_shards(sizes):
    n_x, n_z, n_y, n_c = sizes
    axes = ("rep", "z", "y", "tp")

    def pairs(move):
        found = []
        for x in range(n_x):
            for z in range(n_z):
                for y in range(n_y):
                    for c in range(n_c):
                        to = move(x, z, y, c)
                        if to is not None:
                            a = ((x * n_z + z) * n_y + y) * n_c + c
                            b = ((to[0] * n_z + to[1]) * n_y + to[2]) * n_c + to[3]
                            found.append((a, b))
        return found

    over_x = pairs(lambda x, z, y, c: (1 - x, z, y, c))
    over_y = pairs(lambda x, z, y, c: (x, z, 1 - y, c))
    over_d = pairs(lambda x, z, y, c: (1 - x, z, 1 - y, c))
    over_c = pairs(lambda x, z, y, c: (x, z, y, 1 - c))
    up_z = pairs(lambda x, z, y, c: (x, z + 1, y, c) if z + 1 < n_z else None)
    down_z = pairs(lambda x, z, y, c: (x, z - 1, y, c) if z > 0 else None)
    up_z2 = pairs(lambda x, z, y, c: (x, z + 1, y, c) if 1 <= z < n_z - 1 else None)
    down_z2 = pairs(lambda x, z, y, c: (x, z - 1, y, c) if 0 < z < n_z - 1 else None)
    up_z3 = pairs(lambda x, z, y, c: (x, z + 1, y, c) if z == n_z - 2 else None)
    down_z3 = pairs(lambda x, z, y, c: (x, z - 1, y, c) if z == 1 else None)

    def move(value, perm):
        return lax.ppermute(value, axes, perm)

    def gather(own, received):
        slot = jnp.concatenate([own, received], axis=0)
        r1 = move(slot, up_z)
        l1 = move(slot, down_z)
        r2 = move(r1, up_z2)
        l2 = move(l1, down_z2)
        r3 = move(r2, up_z3)
        l3 = move(l2, down_z3)
        return slot, r1, l1, r2, l2, r3, l3

    def shards(
        incoming_features,
        attend_prenormal_scale,
        probe_matrix,
        lookup_matrix,
        content_matrix,
        forgetting_matrix,
        result_switch_matrix,
        forgetting_shift,
        spike_forget_logarithm,
        attend_unit_scale,
        attend_result_matrix,
        perceptron_scale,
        content_expand_matrix,
        switch_expand_matrix,
        content_kernel,
        switch_kernel,
        contract_matrix,
    ):
        x, z, y, c = (lax.axis_index(axis) for axis in axes)
        quarter = 2 * x + y
        pos = jnp.stack(
            [
                quarter,
                2 * x + (1 - y),
                2 * (1 - x) + y,
                2 * x + (1 - y),
                2 * (1 - x) + (1 - y),
                c,
                z,
                y,
                jnp.int32(n_z - 1),
            ]
        ).astype(jnp.int32)
        span, width = incoming_features.shape
        embed = width * n_c
        chunk = probe_matrix.shape[0]
        part = attend_result_matrix.shape[0] // 4
        pack_rows = 3 * chunk + 2 * part + chunk // 2
        own, send = call(
            pack_kernel,
            [((pack_rows, LANES), BF16)] * 2,
            (
                pos,
                probe_matrix,
                lookup_matrix,
                content_matrix,
                forgetting_matrix,
                result_switch_matrix,
                attend_result_matrix,
            ),
        )
        spike_o, to_x, to_y, to_d = call(
            input_kernel,
            [((span, LANES), BF16)] + [((span, width + LANES), BF16)] * 3,
            (pos, spike_forget_logarithm, incoming_features),
        )
        attn = gather(own, move(send, over_y))
        from_x = move(to_x, over_x)
        from_y = move(to_y, over_y)
        from_d = move(to_d, over_d)

        ff = content_expand_matrix.shape[1] // 4

        def up_part(index):
            return jnp.concatenate(
                [
                    lax.dynamic_slice_in_dim(content_expand_matrix, index * ff, ff, 1),
                    lax.dynamic_slice_in_dim(switch_expand_matrix, index * ff, ff, 1),
                ],
                axis=1,
            )

        def down_part(index):
            return lax.dynamic_slice_in_dim(contract_matrix, index * ff, ff, 0)

        across = 2 * x + (1 - y)
        up = gather(up_part(quarter), move(up_part(across), over_y))
        down = gather(down_part(quarter), move(down_part(across), over_y))

        def halves(blocks):
            mine = jnp.concatenate(blocks, axis=0)
            return mine, move(mine, over_c)

        def reduce(keep, other):
            total = (keep.astype(F32) + other.astype(F32)).astype(BF16)
            blocks = [total[i * span : (i + 1) * span] for i in range(4)]
            return (
                blocks[0], move(blocks[1], over_x), move(blocks[2], over_y), move(blocks[3], over_d)
            )

        def add_up(base, parts):
            total = parts[0].astype(F32)
            for part_ in parts[1:]:
                total = total + part_.astype(F32)
            return (base.astype(F32) + total.astype(BF16).astype(F32)).astype(BF16)

        tokens = 4 * span
        mine, theirs = halves(
            [incoming_features] + [value[:, :width] for value in (from_x, from_y, from_d)],
        )
        key_w = forgetting_shift.shape[0] // 4
        val_w = attend_unit_scale.shape[0] // 4
        shift = lax.dynamic_slice_in_dim(forgetting_shift, quarter * key_w, key_w, 0)
        shift = jnp.concatenate([shift, shift]).reshape(1, LANES)
        unit = lax.dynamic_slice_in_dim(attend_unit_scale, quarter * val_w, val_w, 0)
        keep, other = call(
            attend_kernel,
            [((tokens, width), BF16)] * 2,
            (
                pos,
                mine,
                theirs,
                attend_prenormal_scale.reshape(1, embed),
                shift,
                unit.reshape(1, val_w),
                spike_o,
                from_x,
                from_y,
                from_d,
            )
            + attn,
            scratch=[
                pltpu.VMEM((embed, LANES), BF16),
                pltpu.VMEM((embed, 2 * LANES), BF16),
                pltpu.VMEM((embed, LANES), BF16),
                pltpu.VMEM((8, part, embed // 8), BF16),
                pltpu.VMEM((8, chunk // 2, LANES), BF16),
                pltpu.VMEM((tokens, LANES), F32),
                pltpu.VMEM((tokens, LANES), BF16),
                pltpu.VMEM((tokens, LANES), BF16),
                pltpu.VMEM((tokens, LANES), F32),
                pltpu.VMEM((tokens, LANES), BF16),
                pltpu.SemaphoreType.DMA((48,)),
            ],
            flops=10**10,
            free=7,
        )
        middle = add_up(incoming_features, reduce(keep, move(other, over_c)))
        mine, theirs = halves(
            [middle, move(middle, over_x), move(middle, over_y), move(middle, over_d)],
        )
        taps_v = lax.dynamic_slice_in_dim(content_kernel, quarter * ff, ff, 1)
        taps_g = lax.dynamic_slice_in_dim(switch_kernel, quarter * ff, ff, 1)
        (hidden,) = call(
            expand_kernel,
            [((tokens, ff), BF16)],
            (pos, mine, theirs, perceptron_scale.reshape(1, embed), taps_v, taps_g) + up,
            scratch=[pltpu.VMEM((embed, 2 * ff), BF16), pltpu.SemaphoreType.DMA((8,))],
            flops=10**10,
            free=7,
        )
        half = width // 2
        slot_o, slot_r1, slot_l1, slot_r2, slot_l2, slot_r3, slot_l3 = down
        parts = []
        for kernel, slots in (
            (contract_kernel_one, (slot_o, slot_r2, slot_l2)),
            (contract_kernel_two, (slot_r1, slot_l1, slot_r3, slot_l3)),
        ):
            keep, other = call(
                kernel,
                [((tokens, half), BF16)] * 2,
                (pos, hidden) + slots,
                scratch=[
                    pltpu.VMEM((2, 2, ff, embed // 8), BF16),
                    pltpu.SemaphoreType.DMA((4,)),
                ],
                flops=10**10,
                free=len(slots),
            )
            pieces = reduce(keep, move(other, over_c))
            total = pieces[0].astype(F32)
            for piece in pieces[1:]:
                total = total + piece.astype(F32)
            parts.append(total.astype(BF16).astype(F32))
        even = lax.rem(z, 2) == 0
        ffn = jnp.concatenate(
            [jnp.where(even, parts[0], parts[1]), jnp.where(even, parts[1], parts[0])], axis=1
        )
        return (middle.astype(F32) + ffn).astype(BF16)

    return shards


def plane_sizes(mesh):
    if tuple(mesh.axis_names) != ("rep", "fs", "tp"):
        return None
    n_x, n_fs, n_c = (mesh.shape[axis] for axis in ("rep", "fs", "tp"))
    if n_x != 2 or n_c != 2 or n_fs % 2 or n_fs // 2 != 4:
        return None
    return (n_x, n_fs // 2, 2, n_c)


def solution(mesh):
    sizes = plane_sizes(mesh)
    if sizes is None:
        body, seq = general_shards, ("rep", "fs")
        weight = ("fs",)
        used = mesh
    else:
        body, seq = plane_shards(sizes), ("rep", "z", "y")
        weight = ("z", "y")
        used = Mesh(mesh.devices.reshape(sizes), ("rep", "z", "y", "tp"))
    placed = (
        P(seq, "tp"),
        P(),
        P(weight, "tp"),
        P(weight, "tp"),
        P(weight, "tp"),
        P(weight, "tp"),
        P(weight, "tp"),
        P("tp"),
        P(seq, "tp"),
        P("tp"),
        P("tp", weight),
        P(),
        P(weight, "tp"),
        P(weight, "tp"),
        P(None, "tp"),
        P(None, "tp"),
        P("tp", weight),
    )
    return jax.shard_map(body, mesh=used, in_specs=placed, out_specs=P(seq, "tp"), check_vma=False)
```

profile of v0, /device:TPU:0, one launch (start us, length us, event | category | flops | bytes accessed | tf_op | source)
XLA Modules:
  0.0 254.3 jit_solution(16024879287957143634)
XLA Ops:
  0.6 2.3 shard_map.164
  3.0 3.0 %collective-permute-start.4 = (bf16[1152,128]{1,0:T(8,128)(2,1)}, bf16[1152,128]{1,0:T(8,128)(2,1)S(1)}, u32[]{:S(2)}, u32[]{:S(2)}) collective-permute-start(bf16[1152,128]{1,0:T(8,128)(2,1)} %get-tuple-element.22), channel_id=1, source_target_pairs={{0,2},{1,3},{2,0},{3,1},{4,6},{5,7},{6,4},{7,5},{8,10},{9,11},{10,... | collective-permute-start | bytes 884744 | tf_op jit(solution)/shard_map/ppermute | solution.py:640
  6.0 2.9 %shard_map.163 = (bf16[192,128]{1,0:T(8,128)(2,1)}, bf16[192,1152]{1,0:T(8,128)(2,1)}, bf16[192,1152]{1,0:T(8,128)(2,1)}, bf16[192,1152]{1,0:T(8,128)(2,1)}) custom-call(s32[9]{0:T(128)} %stack.32.pos, f32[192,256]{1,0:T(8,128)} %spike.1, bf16[192,1024]{1,0:T(8,128)(2,1)} %feat.1), custom_call_target="tpu_custom_call" | custom-call | bytes 1048576 | tf_op jit(solution)/shard_map/pallas_call | solution.py:600
  8.9 1.5 collective-permute-start
  15.3 4.6 %collective-permute-start.5 = (bf16[2304,128]{1,0:T(8,128)(2,1)S(1)}, bf16[2304,128]{1,0:T(8,128)(2,1)S(1)}, u32[]{:S(2)}, u32[]{:S(2)}) collective-permute-start(bf16[2304,128]{1,0:T(8,128)(2,1)S(1)} %constant_dynamic-update-slice_fusion.slot_o), channel_id=1, source_target_pairs={{0,4},{1,5},{2,6},{3,7},{4,8},{5,9},{6,10},{7,11},{8,12},{9,13},{1... | collective-permute-start | bytes 1769480 | tf_op jit(solution)/shard_map/ppermute | solution.py:640
  19.9 2.3 collective-permute-done.spike_x
  22.2 10.0 %collective-permute-done.1.spike_y = bf16[192,1152]{1,0:T(8,128)(2,1)S(1)} collective-permute-done((bf16[192,1152]{1,0:T(8,128)(2,1)}, bf16[192,1152]{1,0:T(8,128)(2,1)S(1)}, u32[]{:S(2)}, u32[]{:S(2)}) %collective-permute-start.1) | collective-permute-done | bytes 442400 | tf_op jit(solution)/shard_map/ppermute | solution.py:640
  35.2 15.6 %collective-permute-done.8.slot_l2 = bf16[2304,128]{1,0:T(8,128)(2,1)S(1)} collective-permute-done((bf16[2304,128]{1,0:T(8,128)(2,1)S(1)}, bf16[2304,128]{1,0:T(8,128)(2,1)S(1)}, u32[]{:S(2)}, u32[]{:S(2)}) %collective-permute-start.8) | collective-permute-done | bytes 589856 | tf_op jit(solution)/shard_map/ppermute | solution.py:640
  52.1 1.5 collective-permute-start.9
  55.5 12.2 %collective-permute-done.10.slot_l3 = bf16[2304,128]{1,0:T(8,128)(2,1)} collective-permute-done((bf16[2304,128]{1,0:T(8,128)(2,1)S(1)}, bf16[2304,128]{1,0:T(8,128)(2,1)}, u32[]{:S(2)}, u32[]{:S(2)}) %collective-permute-start.10) | collective-permute-done | bytes 589856 | tf_op jit(solution)/shard_map/ppermute | solution.py:640
  67.7 17.0 %shard_map.165 = (bf16[768,1024]{1,0:T(8,128)(2,1)}, bf16[768,1024]{1,0:T(8,128)(2,1)}) custom-call(s32[9]{0:T(128)} %stack.32.pos, bf16[768,1024]{1,0:T(8,128)(2,1)} %copy-done.3, bf16[768,1024]{1,0:T(8,128)(2,1)} %collective-permute-done.3.theirs, bf16[1,2048]{1,0:T(2,128)(2,1)} %reshape.12.scale, f32[1,128]{1,0:T(1,128)} %maximum_bitcast_fusion.shift, ...), custom_call_target="tpu_custom_call" | custom-call | flops 10000000000 | bytes 1048576 | tf_op jit(solution)/shard_map/pallas_call | solution.py:600
  86.1 1.7 collective-permute-start.19
  87.7 12.7 %collective-permute-done.19 = bf16[256,1024]{1,0:T(8,128)(2,1)S(1)} collective-permute-done((bf16[256,1024]{1,0:T(8,128)(2,1)S(1)}, bf16[256,1024]{1,0:T(8,128)(2,1)S(1)}, u32[]{:S(2)}, u32[]{:S(2)}) %collective-permute-start.19) | collective-permute-done | bytes 524320 | tf_op jit(solution)/shard_map/ppermute | solution.py:640
  104.1 1.6 collective-permute-start.12
  105.7 1.5 collective-permute-start.13
  107.6 8.5 %collective-permute-done.12 = bf16[192,1024]{1,0:T(8,128)(2,1)S(1)} collective-permute-done((bf16[192,1024]{1,0:T(8,128)(2,1)S(1)}, bf16[192,1024]{1,0:T(8,128)(2,1)S(1)}, u32[]{:S(2)}, u32[]{:S(2)}) %collective-permute-start.12) | collective-permute-done | bytes 393248 | tf_op jit(solution)/shard_map/ppermute | solution.py:640
  116.1 8.3 %collective-permute-done.13 = bf16[192,1024]{1,0:T(8,128)(2,1)S(1)} collective-permute-done((bf16[192,1024]{1,0:T(8,128)(2,1)S(1)}, bf16[192,1024]{1,0:T(8,128)(2,1)S(1)}, u32[]{:S(2)}, u32[]{:S(2)}) %collective-permute-start.13) | collective-permute-done | bytes 393248 | tf_op jit(solution)/shard_map/ppermute | solution.py:640
  131.4 5.5 %collective-permute-done.15 = bf16[192,1024]{1,0:T(8,128)(2,1)S(1)} collective-permute-done((bf16[192,1024]{1,0:T(8,128)(2,1)S(1)}, bf16[192,1024]{1,0:T(8,128)(2,1)S(1)}, u32[]{:S(2)}, u32[]{:S(2)}) %collective-permute-start.15) | collective-permute-done | bytes 393248 | tf_op jit(solution)/shard_map/ppermute | solution.py:640
  136.9 7.1 %collective-permute-done.16 = bf16[192,1024]{1,0:T(8,128)(2,1)S(1)} collective-permute-done((bf16[192,1024]{1,0:T(8,128)(2,1)S(1)}, bf16[192,1024]{1,0:T(8,128)(2,1)S(1)}, u32[]{:S(2)}, u32[]{:S(2)}) %collective-permute-start.16) | collective-permute-done | bytes 393248 | tf_op jit(solution)/shard_map/ppermute | solution.py:640
  144.9 8.1 %collective-permute-done.26 = bf16[512,256]{1,0:T(8,128)(2,1)S(1)} collective-permute-done((bf16[512,256]{1,0:T(8,128)(2,1)S(1)}, bf16[512,256]{1,0:T(8,128)(2,1)S(1)}, u32[]{:S(2)}, u32[]{:S(2)}) %collective-permute-start.26) | collective-permute-done | bytes 262176 | tf_op jit(solution)/shard_map/ppermute | solution.py:640
  153.1 5.6 %collective-permute-start.27 = (bf16[1024,256]{1,0:T(8,128)(2,1)S(1)}, bf16[1024,256]{1,0:T(8,128)(2,1)S(1)}, u32[]{:S(2)}, u32[]{:S(2)}) collective-permute-start(bf16[1024,256]{1,0:T(8,128)(2,1)S(1)} %pad_maximum_fusion.4.slot_o), channel_id=1, source_target_pairs={{0,4},{1,5},{2,6},{3,7},{4,8},{5,9},{6,10},{7,11},{8,12},{9,13},{1... | collective-permute-start | bytes 1572872 | tf_op jit(solution)/shard_map/ppermute | solution.py:640
  162.1 7.5 %collective-permute-done.27.slot_r1 = bf16[1024,256]{1,0:T(8,128)(2,1)S(1)} collective-permute-done((bf16[1024,256]{1,0:T(8,128)(2,1)S(1)}, bf16[1024,256]{1,0:T(8,128)(2,1)S(1)}, u32[]{:S(2)}, u32[]{:S(2)}) %collective-permute-start.27) | collective-permute-done | bytes 524320 | tf_op jit(solution)/shard_map/ppermute | solution.py:640
  170.3 5.6 %collective-permute-done.29.slot_l1 = bf16[1024,256]{1,0:T(8,128)(2,1)S(1)} collective-permute-done((bf16[1024,256]{1,0:T(8,128)(2,1)S(1)}, bf16[1024,256]{1,0:T(8,128)(2,1)S(1)}, u32[]{:S(2)}, u32[]{:S(2)}) %collective-permute-start.29) | collective-permute-done | bytes 524320 | tf_op jit(solution)/shard_map/ppermute | solution.py:640
  180.8 27.5 %collective-permute-done.30.slot_l2 = bf16[1024,256]{1,0:T(8,128)(2,1)S(1)} collective-permute-done((bf16[1024,256]{1,0:T(8,128)(2,1)S(1)}, bf16[1024,256]{1,0:T(8,128)(2,1)S(1)}, u32[]{:S(2)}, u32[]{:S(2)}) %collective-permute-start.30) | collective-permute-done | bytes 524320 | tf_op jit(solution)/shard_map/ppermute | solution.py:640
  211.5 11.1 %shard_map.166.hidden = bf16[768,512]{1,0:T(8,128)(2,1)} custom-call(s32[9]{0:T(128)} %stack.32.pos, bf16[768,1024]{1,0:T(8,128)(2,1)} %copy-done.2, bf16[768,1024]{1,0:T(8,128)(2,1)} %copy-done.17, bf16[1,2048]{1,0:T(2,128)(2,1)} %reshape.15.scale, bf16[3,512]{1,0:T(4,128)(2,1)} %get-tuple-element.50.taps_v, bf16[3,512]{1,0:T(4,128)(2,1)} %get-tuple-element.49.taps_g, ...), custom_call_target="tpu_custom_call" | custom-call | flops 10000000000 | bytes 1048576 | tf_op jit(solution)/shard_map/pallas_call | solution.py:600
  222.9 4.3 %shard_map.168 = (bf16[768,512]{1,0:T(8,128)(2,1)}, bf16[768,512]{1,0:T(8,128)(2,1)}) custom-call(s32[9]{0:T(128)} %stack.32.pos, bf16[768,512]{1,0:T(8,128)(2,1)} %shard_map.166.hidden, bf16[1024,256]{1,0:T(8,128)(2,1)} %copy-done.28, bf16[1024,256]{1,0:T(8,128)(2,1)} %copy-done.29, bf16[1024,256]{1,0:T(8,128)(2,1)} %collective-permute-done.35.slot_r3, ...), custom_call_target="tpu_custom_call" | custom-call | flops 10000000000 | bytes 1048576 | tf_op jit(solution)/shard_map/pallas_call | solution.py:600
  227.3 4.3 %shard_map.167 = (bf16[768,512]{1,0:T(8,128)(2,1)}, bf16[768,512]{1,0:T(8,128)(2,1)}) custom-call(s32[9]{0:T(128)} %stack.32.pos, bf16[768,512]{1,0:T(8,128)(2,1)} %shard_map.166.hidden, bf16[1024,256]{1,0:T(8,128)(2,1)} %copy-done.8, bf16[1024,256]{1,0:T(8,128)(2,1)} %copy-done.30, bf16[1024,256]{1,0:T(8,128)(2,1)} %copy-done.31), custom_call_target="tpu_custom_call" | custom-call | flops 10000000000 | bytes 1048576 | tf_op jit(solution)/shard_map/pallas_call | solution.py:600
  234.2 1.8 collective-permute-start.40
  238.7 1.5 collective-permute-done.38
  241.4 3.2 %collective-permute-done.39 = bf16[192,512]{1,0:T(8,128)(2,1)S(1)} collective-permute-done((bf16[192,512]{1,0:T(8,128)(2,1)S(1)}, bf16[192,512]{1,0:T(8,128)(2,1)S(1)}, u32[]{:S(2)}, u32[]{:S(2)}) %collective-permute-start.39) | collective-permute-done | bytes 196640 | tf_op jit(solution)/shard_map/ppermute | solution.py:640
  244.6 4.1 %collective-permute-done.32 = bf16[192,512]{1,0:T(8,128)(2,1)S(1)} collective-permute-done((bf16[192,512]{1,0:T(8,128)(2,1)}, bf16[192,512]{1,0:T(8,128)(2,1)S(1)}, u32[]{:S(2)}, u32[]{:S(2)}) %collective-permute-start.32) | collective-permute-done | bytes 196640 | tf_op jit(solution)/shard_map/ppermute | solution.py:640
  248.7 3.6 %collective-permute-done.33 = bf16[192,512]{1,0:T(8,128)(2,1)S(1)} collective-permute-done((bf16[192,512]{1,0:T(8,128)(2,1)}, bf16[192,512]{1,0:T(8,128)(2,1)S(1)}, u32[]{:S(2)}, u32[]{:S(2)}) %collective-permute-start.33) | collective-permute-done | bytes 196640 | tf_op jit(solution)/shard_map/ppermute | solution.py:640
  (151 shorter events, 45.5 us)
Async XLA Ops:
  8.9 13.2 %collective-permute-start = (bf16[192,1152]{1,0:T(8,128)(2,1)}, bf16[192,1152]{1,0:T(8,128)(2,1)S(1)}, u32[]{:S(2)}, u32[]{:S(2)}) collective-permute-start(bf16[192,1152]{1,0:T(8,128)(2,1)} %get-tuple-element.17), channel_id=1, source_target_pairs={{0,16},{1,17},{2,18},{3,19},{4,20},{5,21},{6,22},{7,23},{8,24},{9,... | collective-permute-start | bytes 1327112 | tf_op jit(solution)/shard_map/ppermute | solution.py:640
  10.4 21.8 %collective-permute-start.1 = (bf16[192,1152]{1,0:T(8,128)(2,1)}, bf16[192,1152]{1,0:T(8,128)(2,1)S(1)}, u32[]{:S(2)}, u32[]{:S(2)}) collective-permute-start(bf16[192,1152]{1,0:T(8,128)(2,1)} %get-tuple-element.18), channel_id=1, source_target_pairs={{0,2},{1,3},{2,0},{3,1},{4,6},{5,7},{6,4},{7,5},{8,10},{9,11},{10,... | collective-permute-start | bytes 1327112 | tf_op jit(solution)/shard_map/ppermute | solution.py:640
  10.9 21.3 %collective-permute-start.2 = (bf16[192,1152]{1,0:T(8,128)(2,1)}, bf16[192,1152]{1,0:T(8,128)(2,1)S(1)}, u32[]{:S(2)}, u32[]{:S(2)}) collective-permute-start(bf16[192,1152]{1,0:T(8,128)(2,1)} %get-tuple-element.19), channel_id=1, source_target_pairs={{0,18},{1,19},{2,16},{3,17},{4,22},{5,23},{6,20},{7,21},{8,26},{9,... | collective-permute-start | bytes 1327112 | tf_op jit(solution)/shard_map/ppermute | solution.py:640
  14.0 19.1 %collective-permute-start.6 = (bf16[2304,128]{1,0:T(8,128)(2,1)S(1)}, bf16[2304,128]{1,0:T(8,128)(2,1)S(1)}, u32[]{:S(2)}, u32[]{:S(2)}) collective-permute-start(bf16[2304,128]{1,0:T(8,128)(2,1)S(1)} %constant_dynamic-update-slice_fusion.slot_o), channel_id=1, source_target_pairs={{4,0},{5,1},{6,2},{7,3},{8,4},{9,5},{10,6},{11,7},{12,8},{13,9},{1... | collective-permute-start | bytes 1769480 | tf_op jit(solution)/shard_map/ppermute | solution.py:640
  15.3 19.2 %collective-permute-start.5 = (bf16[2304,128]{1,0:T(8,128)(2,1)S(1)}, bf16[2304,128]{1,0:T(8,128)(2,1)S(1)}, u32[]{:S(2)}, u32[]{:S(2)}) collective-permute-start(bf16[2304,128]{1,0:T(8,128)(2,1)S(1)} %constant_dynamic-update-slice_fusion.slot_o), channel_id=1, source_target_pairs={{0,4},{1,5},{2,6},{3,7},{4,8},{5,9},{6,10},{7,11},{8,12},{9,13},{1... | collective-permute-start | bytes 1769480 | tf_op jit(solution)/shard_map/ppermute | solution.py:640
  33.1 22.4 %collective-permute-start.3 = (bf16[768,1024]{1,0:T(8,128)(2,1)S(1)}, bf16[768,1024]{1,0:T(8,128)(2,1)}, u32[]{:S(2)}, u32[]{:S(2)}) collective-permute-start(bf16[768,1024]{1,0:T(8,128)(2,1)S(1)} %pad_maximum_fusion.mine), channel_id=1, source_target_pairs={{0,1},{1,0},{2,3},{3,2},{4,5},{5,4},{6,7},{7,6},{8,9},{9,8},{10,11... | collective-permute-start | bytes 4718600 | tf_op jit(solution)/shard_map/ppermute | solution.py:640
  33.1 17.7 %collective-permute-start.8 = (bf16[2304,128]{1,0:T(8,128)(2,1)S(1)}, bf16[2304,128]{1,0:T(8,128)(2,1)S(1)}, u32[]{:S(2)}, u32[]{:S(2)}) collective-permute-start(bf16[2304,128]{1,0:T(8,128)(2,1)S(1)} %collective-permute-done.6.slot_l1), channel_id=1, source_target_pairs={{4,0},{5,1},{6,2},{7,3},{8,4},{9,5},{10,6},{11,7},{20,16},{21,17},... | collective-permute-start | bytes 1769480 | tf_op jit(solution)/shard_map/ppermute | solution.py:640
  34.4 17.6 %collective-permute-start.7 = (bf16[2304,128]{1,0:T(8,128)(2,1)S(1)}, bf16[2304,128]{1,0:T(8,128)(2,1)S(1)}, u32[]{:S(2)}, u32[]{:S(2)}) collective-permute-start(bf16[2304,128]{1,0:T(8,128)(2,1)S(1)} %collective-permute-done.5.slot_r1), channel_id=1, source_target_pairs={{4,8},{5,9},{6,10},{7,11},{8,12},{9,13},{10,14},{11,15},{20,24},{2... | collective-permute-start | bytes 1769480 | tf_op jit(solution)/shard_map/ppermute | solution.py:640
  50.8 16.9 %collective-permute-start.10 = (bf16[2304,128]{1,0:T(8,128)(2,1)S(1)}, bf16[2304,128]{1,0:T(8,128)(2,1)}, u32[]{:S(2)}, u32[]{:S(2)}) collective-permute-start(bf16[2304,128]{1,0:T(8,128)(2,1)S(1)} %collective-permute-done.8.slot_l2), channel_id=1, source_target_pairs={{4,0},{5,1},{6,2},{7,3},{20,16},{21,17},{22,18},{23,19}} | collective-permute-start | bytes 1769480 | tf_op jit(solution)/shard_map/ppermute | solution.py:640
  52.1 15.6 %collective-permute-start.9 = (bf16[2304,128]{1,0:T(8,128)(2,1)S(1)}, bf16[2304,128]{1,0:T(8,128)(2,1)}, u32[]{:S(2)}, u32[]{:S(2)}) collective-permute-start(bf16[2304,128]{1,0:T(8,128)(2,1)S(1)} %collective-permute-done.7.slot_r2), channel_id=1, source_target_pairs={{8,12},{9,13},{10,14},{11,15},{24,28},{25,29},{26,30},{27,31}} | collective-permute-start | bytes 1769480 | tf_op jit(solution)/shard_map/ppermute | solution.py:640
  84.8 18.5 %collective-permute-start.11 = (bf16[768,1024]{1,0:T(8,128)(2,1)}, bf16[768,1024]{1,0:T(8,128)(2,1)S(1)}, u32[]{:S(2)}, u32[]{:S(2)}) collective-permute-start(bf16[768,1024]{1,0:T(8,128)(2,1)} %get-tuple-element.24), channel_id=1, source_target_pairs={{0,1},{1,0},{2,3},{3,2},{4,5},{5,4},{6,7},{7,6},{8,9},{9,8},{10,11... | collective-permute-start | bytes 4718600 | tf_op jit(solution)/shard_map/ppermute | solution.py:640
  86.1 14.4 %collective-permute-start.19 = (bf16[256,1024]{1,0:T(8,128)(2,1)S(1)}, bf16[256,1024]{1,0:T(8,128)(2,1)S(1)}, u32[]{:S(2)}, u32[]{:S(2)}) collective-permute-start(bf16[256,1024]{1,0:T(8,128)(2,1)S(1)} %pad_maximum_fusion.3), channel_id=1, source_target_pairs={{0,2},{1,3},{2,0},{3,1},{4,6},{5,7},{6,4},{7,5},{8,10},{9,11},{10,... | collective-permute-start | bytes 1572872 | tf_op jit(solution)/shard_map/ppermute | solution.py:640
  100.5 27.8 %collective-permute-start.20 = (bf16[512,1024]{1,0:T(8,128)(2,1)S(1)}, bf16[512,1024]{1,0:T(8,128)(2,1)S(1)}, u32[]{:S(2)}, u32[]{:S(2)}) collective-permute-start(bf16[512,1024]{1,0:T(8,128)(2,1)S(1)} %pad_maximum_fusion.2.slot_o), channel_id=1, source_target_pairs={{0,4},{1,5},{2,6},{3,7},{4,8},{5,9},{6,10},{7,11},{8,12},{9,13},{1... | collective-permute-start | bytes 3145736 | tf_op jit(solution)/shard_map/ppermute | solution.py:640
  102.0 28.1 %collective-permute-start.21 = (bf16[512,1024]{1,0:T(8,128)(2,1)S(1)}, bf16[512,1024]{1,0:T(8,128)(2,1)S(1)}, u32[]{:S(2)}, u32[]{:S(2)}) collective-permute-start(bf16[512,1024]{1,0:T(8,128)(2,1)S(1)} %pad_maximum_fusion.2.slot_o), channel_id=1, source_target_pairs={{4,0},{5,1},{6,2},{7,3},{8,4},{9,5},{10,6},{11,7},{12,8},{13,9},{1... | collective-permute-start | bytes 3145736 | tf_op jit(solution)/shard_map/ppermute | solution.py:640
  104.1 12.1 %collective-permute-start.12 = (bf16[192,1024]{1,0:T(8,128)(2,1)S(1)}, bf16[192,1024]{1,0:T(8,128)(2,1)S(1)}, u32[]{:S(2)}, u32[]{:S(2)}) collective-permute-start(bf16[192,1024]{1,0:T(8,128)(2,1)S(1)} %get-tuple-element.32), channel_id=1, source_target_pairs={{0,16},{1,17},{2,18},{3,19},{4,20},{5,21},{6,22},{7,23},{8,24},{9,... | collective-permute-start | bytes 1179656 | tf_op jit(solution)/shard_map/ppermute | solution.py:640
  105.7 18.8 %collective-permute-start.13 = (bf16[192,1024]{1,0:T(8,128)(2,1)S(1)}, bf16[192,1024]{1,0:T(8,128)(2,1)S(1)}, u32[]{:S(2)}, u32[]{:S(2)}) collective-permute-start(bf16[192,1024]{1,0:T(8,128)(2,1)S(1)} %get-tuple-element.34), channel_id=1, source_target_pairs={{0,2},{1,3},{2,0},{3,1},{4,6},{5,7},{6,4},{7,5},{8,10},{9,11},{10,... | collective-permute-start | bytes 1179656 | tf_op jit(solution)/shard_map/ppermute | solution.py:640
  107.2 17.2 %collective-permute-start.14 = (bf16[192,1024]{1,0:T(8,128)(2,1)S(1)}, bf16[192,1024]{1,0:T(8,128)(2,1)S(1)}, u32[]{:S(2)}, u32[]{:S(2)}) collective-permute-start(bf16[192,1024]{1,0:T(8,128)(2,1)S(1)} %get-tuple-element.33), channel_id=1, source_target_pairs={{0,18},{1,19},{2,16},{3,17},{4,22},{5,23},{6,20},{7,21},{8,26},{9,... | collective-permute-start | bytes 1179656 | tf_op jit(solution)/shard_map/ppermute | solution.py:640
  124.8 12.1 %collective-permute-start.15 = (bf16[192,1024]{1,0:T(8,128)(2,1)S(1)}, bf16[192,1024]{1,0:T(8,128)(2,1)S(1)}, u32[]{:S(2)}, u32[]{:S(2)}) collective-permute-start(bf16[192,1024]{1,0:T(8,128)(2,1)S(1)} %add_convert_fusion.3), channel_id=1, source_target_pairs={{0,16},{1,17},{2,18},{3,19},{4,20},{5,21},{6,22},{7,23},{8,24},{9,... | collective-permute-start | bytes 1179656 | tf_op jit(solution)/shard_map/ppermute | solution.py:640
  126.1 17.9 %collective-permute-start.16 = (bf16[192,1024]{1,0:T(8,128)(2,1)S(1)}, bf16[192,1024]{1,0:T(8,128)(2,1)S(1)}, u32[]{:S(2)}, u32[]{:S(2)}) collective-permute-start(bf16[192,1024]{1,0:T(8,128)(2,1)S(1)} %add_convert_fusion.3), channel_id=1, source_target_pairs={{0,2},{1,3},{2,0},{3,1},{4,6},{5,7},{6,4},{7,5},{8,10},{9,11},{10,... | collective-permute-start | bytes 1179656 | tf_op jit(solution)/shard_map/ppermute | solution.py:640
  126.9 17.1 %collective-permute-start.17 = (bf16[192,1024]{1,0:T(8,128)(2,1)S(1)}, bf16[192,1024]{1,0:T(8,128)(2,1)S(1)}, u32[]{:S(2)}, u32[]{:S(2)}) collective-permute-start(bf16[192,1024]{1,0:T(8,128)(2,1)S(1)} %add_convert_fusion.3), channel_id=1, source_target_pairs={{0,18},{1,19},{2,16},{3,17},{4,22},{5,23},{6,20},{7,21},{8,26},{9,... | collective-permute-start | bytes 1179656 | tf_op jit(solution)/shard_map/ppermute | solution.py:640
  128.4 31.6 %collective-permute-start.22 = (bf16[512,1024]{1,0:T(8,128)(2,1)S(1)}, bf16[512,1024]{1,0:T(8,128)(2,1)S(1)}, u32[]{:S(2)}, u32[]{:S(2)}) collective-permute-start(bf16[512,1024]{1,0:T(8,128)(2,1)S(1)} %collective-permute-done.20.slot_r1), channel_id=1, source_target_pairs={{4,8},{5,9},{6,10},{7,11},{8,12},{9,13},{10,14},{11,15},{20,24},{2... | collective-permute-start | bytes 3145736 | tf_op jit(solution)/shard_map/ppermute | solution.py:640
  130.1 30.7 %collective-permute-start.23 = (bf16[512,1024]{1,0:T(8,128)(2,1)S(1)}, bf16[512,1024]{1,0:T(8,128)(2,1)S(1)}, u32[]{:S(2)}, u32[]{:S(2)}) collective-permute-start(bf16[512,1024]{1,0:T(8,128)(2,1)S(1)} %collective-permute-done.21.slot_l1), channel_id=1, source_target_pairs={{4,0},{5,1},{6,2},{7,3},{8,4},{9,5},{10,6},{11,7},{20,16},{21,17},... | collective-permute-start | bytes 3145736 | tf_op jit(solution)/shard_map/ppermute | solution.py:640
  144.2 65.5 %collective-permute-start.18 = (bf16[768,1024]{1,0:T(8,128)(2,1)S(1)}, bf16[768,1024]{1,0:T(8,128)(2,1)S(1)}, u32[]{:S(2)}, u32[]{:S(2)}) collective-permute-start(bf16[768,1024]{1,0:T(8,128)(2,1)S(1)} %pad_maximum_fusion.1.mine), channel_id=1, source_target_pairs={{0,1},{1,0},{2,3},{3,2},{4,5},{5,4},{6,7},{7,6},{8,9},{9,8},{10,11... | collective-permute-start | bytes 4718600 | tf_op jit(solution)/shard_map/ppermute | solution.py:640
  153.1 16.5 %collective-permute-start.27 = (bf16[1024,256]{1,0:T(8,128)(2,1)S(1)}, bf16[1024,256]{1,0:T(8,128)(2,1)S(1)}, u32[]{:S(2)}, u32[]{:S(2)}) collective-permute-start(bf16[1024,256]{1,0:T(8,128)(2,1)S(1)} %pad_maximum_fusion.4.slot_o), channel_id=1, source_target_pairs={{0,4},{1,5},{2,6},{3,7},{4,8},{5,9},{6,10},{7,11},{8,12},{9,13},{1... | collective-permute-start | bytes 1572872 | tf_op jit(solution)/shard_map/ppermute | solution.py:640
  158.7 17.2 %collective-permute-start.29 = (bf16[1024,256]{1,0:T(8,128)(2,1)S(1)}, bf16[1024,256]{1,0:T(8,128)(2,1)S(1)}, u32[]{:S(2)}, u32[]{:S(2)}) collective-permute-start(bf16[1024,256]{1,0:T(8,128)(2,1)S(1)} %pad_maximum_fusion.4.slot_o), channel_id=1, source_target_pairs={{4,0},{5,1},{6,2},{7,3},{8,4},{9,5},{10,6},{11,7},{12,8},{13,9},{1... | collective-permute-start | bytes 1572872 | tf_op jit(solution)/shard_map/ppermute | solution.py:640
  160.0 49.6 %collective-permute-start.24 = (bf16[512,1024]{1,0:T(8,128)(2,1)S(1)}, bf16[512,1024]{1,0:T(8,128)(2,1)S(1)}, u32[]{:S(2)}, u32[]{:S(2)}) collective-permute-start(bf16[512,1024]{1,0:T(8,128)(2,1)S(1)} %collective-permute-done.22.slot_r2), channel_id=1, source_target_pairs={{8,12},{9,13},{10,14},{11,15},{24,28},{25,29},{26,30},{27,31}} | collective-permute-start | bytes 3145736 | tf_op jit(solution)/shard_map/ppermute | solution.py:640
  160.8 48.8 %collective-permute-start.25 = (bf16[512,1024]{1,0:T(8,128)(2,1)S(1)}, bf16[512,1024]{1,0:T(8,128)(2,1)S(1)}, u32[]{:S(2)}, u32[]{:S(2)}) collective-permute-start(bf16[512,1024]{1,0:T(8,128)(2,1)S(1)} %collective-permute-done.23.slot_l2), channel_id=1, source_target_pairs={{4,0},{5,1},{6,2},{7,3},{20,16},{21,17},{22,18},{23,19}} | collective-permute-start | bytes 3145736 | tf_op jit(solution)/shard_map/ppermute | solution.py:640
  176.0 32.4 %collective-permute-start.30 = (bf16[1024,256]{1,0:T(8,128)(2,1)S(1)}, bf16[1024,256]{1,0:T(8,128)(2,1)S(1)}, u32[]{:S(2)}, u32[]{:S(2)}) collective-permute-start(bf16[1024,256]{1,0:T(8,128)(2,1)S(1)} %collective-permute-done.29.slot_l1), channel_id=1, source_target_pairs={{4,0},{5,1},{6,2},{7,3},{8,4},{9,5},{10,6},{11,7},{20,16},{21,17},... | collective-permute-start | bytes 1572872 | tf_op jit(solution)/shard_map/ppermute | solution.py:640
  179.4 43.2 %collective-permute-start.35 = (bf16[1024,256]{1,0:T(8,128)(2,1)S(1)}, bf16[1024,256]{1,0:T(8,128)(2,1)}, u32[]{:S(2)}, u32[]{:S(2)}) collective-permute-start(bf16[1024,256]{1,0:T(8,128)(2,1)S(1)} %collective-permute-done.28.slot_r2), channel_id=1, source_target_pairs={{8,12},{9,13},{10,14},{11,15},{24,28},{25,29},{26,30},{27,31}} | collective-permute-start | bytes 1572872 | tf_op jit(solution)/shard_map/ppermute | solution.py:640
  208.3 14.6 %collective-permute-start.36 = (bf16[1024,256]{1,0:T(8,128)(2,1)S(1)}, bf16[1024,256]{1,0:T(8,128)(2,1)}, u32[]{:S(2)}, u32[]{:S(2)}) collective-permute-start(bf16[1024,256]{1,0:T(8,128)(2,1)S(1)} %collective-permute-done.30.slot_l2), channel_id=1, source_target_pairs={{4,0},{5,1},{6,2},{7,3},{20,16},{21,17},{22,18},{23,19}} | collective-permute-start | bytes 1572872 | tf_op jit(solution)/shard_map/ppermute | solution.py:640
  237.5 14.7 %collective-permute-start.33 = (bf16[192,512]{1,0:T(8,128)(2,1)}, bf16[192,512]{1,0:T(8,128)(2,1)S(1)}, u32[]{:S(2)}, u32[]{:S(2)}) collective-permute-start(bf16[192,512]{1,0:T(8,128)(2,1)} %get-tuple-element.46), channel_id=1, source_target_pairs={{0,2},{1,3},{2,0},{3,1},{4,6},{5,7},{6,4},{7,5},{8,10},{9,11},{10,... | collective-permute-start | bytes 589832 | tf_op jit(solution)/shard_map/ppermute | solution.py:640
  240.2 12.1 %collective-permute-start.34 = (bf16[192,512]{1,0:T(8,128)(2,1)S(1)}, bf16[192,512]{1,0:T(8,128)(2,1)}, u32[]{:S(2)}, u32[]{:S(2)}) collective-permute-start(bf16[192,512]{1,0:T(8,128)(2,1)S(1)} %get-tuple-element.45), channel_id=1, source_target_pairs={{0,18},{1,19},{2,16},{3,17},{4,22},{5,23},{6,20},{7,21},{8,26},{9,... | collective-permute-start | bytes 589832 | tf_op jit(solution)/shard_map/ppermute | solution.py:640
  (42 other events, 810.4 us)
where the time goes:
time: 255 us; the launch traced here: 254 us
  waiting for transfers between devices  145 us (57%)
  starting transfers between devices  52.2 us (20%)
  Pallas kernels  41.9 us (16%)
  local copies, waits for them, and re-layouts  9.54 us (4%)
  other arithmetic  4.57 us (2%)
    ppermute x41, waiting for transfers between devices, move(): return lax.ppermute(value, axes, perm)  145 us
    ppermute x41, starting transfers between devices, move(): return lax.ppermute(value, axes, perm)  52.2 us
    pallas_call x6, Pallas kernels, call(): pl.pallas_call(kernel, out_shape=[jax.ShapeDtypeStruct(*o) for o in outs]...  41.9 us
  transfers between devices with their start and end apart: 41, of which 20 were waited for; matrix products, arithmetic and copies ran while one was open for 4% of the time, Pallas kernels for 7%

commit v1 on v0

--- a/solution.py
+++ b/solution.py
@@ -493,23 +493,23 @@
 
 def expand_kernel(
     pos, mine, theirs, scale, taps_v, taps_g,
-    slot_o, slot_r1, slot_l1, slot_r2, slot_l2, slot_r3, slot_l3,
-    hidden, w_up, sems,
+    *refs,
 ):
+    own, received = refs[0:7], refs[7:14]
+    hidden, w_up, sems = refs[14:]
     core, y = pos[5], pos[7]
-    chunk = slot_o.shape[0] // 2
+    chunk = own[0].shape[0]
     span = hidden.shape[0] // 4
     width = hidden.shape[1]
 
-    slots = (slot_o, slot_r1, slot_l1, slot_r2, slot_l2, slot_r3, slot_l3)
     waits = []
-    for index, (zi, choices) in enumerate(blocks_of(pos, slots)):
-        for j in range(2):
-            side = y if j == 0 else 1 - y
+    for j, slots in enumerate((own, received)):
+        side = y if j == 0 else 1 - y
+        for index, (zi, choices) in enumerate(blocks_of(pos, slots)):
             dst = w_up.at[pl.ds(pl.multiple_of((zi * 2 + side) * chunk, chunk), chunk), :]
             sem = sems.at[index * 2 + j]
-            copy_from(choices, sem, dst, lambda ref, b=j * chunk: ref.at[pl.ds(b, chunk), :])
-            waits.append((slot_o.at[pl.ds(j * chunk, chunk), :], dst, sem))
+            copy_from(choices, sem, dst, lambda ref: ref)
+            waits.append((slots[0], dst, sem))
     for source, dst, sem in waits:
         pltpu.make_async_copy(source, dst, sem).wait()
 
@@ -546,17 +546,16 @@
     lax.fori_loop(0, 4, sequence, 0)
 
 
-def contract_pair(pos, hidden, blocks, keep, send, weights, sems):
+def contract_pair(pos, hidden, shards, keep, send, weights, sems):
     y = pos[7]
-    rows = weights.shape[2]
     width = weights.shape[3]
     waits = []
-    for index, (where, choices) in enumerate(blocks):
-        for j in range(2):
+    for j, blocks in enumerate(shards):
+        for index, (where, choices) in enumerate(blocks):
             dst = weights.at[where, y if j == 0 else 1 - y]
             sem = sems.at[index * 2 + j]
-            copy_from(choices, sem, dst, lambda ref, b=j * rows: ref.at[pl.ds(b, rows), :])
-            waits.append((choices[0][1].at[pl.ds(j * rows, rows), :], dst, sem))
+            copy_from(choices, sem, dst, lambda ref: ref)
+            waits.append((choices[0][1], dst, sem))
     for source, dst, sem in waits:
         pltpu.make_async_copy(source, dst, sem).wait()
     for index, out in ((1, send), (0, keep)):
@@ -566,34 +565,38 @@
             ).astype(BF16)
 
 
-def contract_kernel_one(pos, hidden, slot_o, slot_r2, slot_l2, keep, send, weights, sems):
+def contract_kernel_one(pos, hidden, *refs):
     z = pos[6]
     same = jnp.where((z // 2) == pos[5], 0, 1)
     low = z < 2
-    blocks = (
-        (same, ((None, slot_o),)),
-        (1 - same, ((low, slot_l2), (jnp.logical_not(low), slot_r2))),
-    )
-    contract_pair(pos, hidden, blocks, keep, send, weights, sems)
-
-
-def contract_kernel_two(
-    pos, hidden, slot_r1, slot_l1, slot_r3, slot_l3, keep, send, weights, sems
-):
+
+    def blocks(slot_o, slot_r2, slot_l2):
+        return (
+            (same, ((None, slot_o),)),
+            (1 - same, ((low, slot_l2), (jnp.logical_not(low), slot_r2))),
+        )
+
+    contract_pair(pos, hidden, (blocks(*refs[0:3]), blocks(*refs[3:6])), *refs[6:])
+
+
+def contract_kernel_two(pos, hidden, *refs):
     z, last = pos[6], pos[8]
     same = jnp.where((z // 2) == pos[5], 0, 1)
     even = lax.rem(z, 2) == 0
-    blocks = (
-        (same, ((even, slot_l1), (jnp.logical_not(even), slot_r1))),
-        (
-            1 - same,
-            ((z == 0, slot_l3), (z == 1, slot_l1), (z == 2, slot_r1), (z == last, slot_r3)),
-        ),
-    )
-    contract_pair(pos, hidden, blocks, keep, send, weights, sems)
-
-
-def call(kernel, outs, args, scratch=(), flops=0, free=0):
+
+    def blocks(slot_r1, slot_l1, slot_r3, slot_l3):
+        return (
+            (same, ((even, slot_l1), (jnp.logical_not(even), slot_r1))),
+            (
+                1 - same,
+                ((z == 0, slot_l3), (z == 1, slot_l1), (z == 2, slot_r1), (z == last, slot_r3)),
+            ),
+        )
+
+    contract_pair(pos, hidden, (blocks(*refs[0:4]), blocks(*refs[4:8])), *refs[8:])
+
+
+def call(kernel, outs, args, scratch=(), flops=0, free=0, grant=24):
     in_specs = [pl.BlockSpec(memory_space=pltpu.SMEM)]
     in_specs += [pl.BlockSpec(memory_space=pltpu.VMEM)] * (len(args) - 1 - free)
     in_specs += [pl.BlockSpec(memory_space=pl.ANY)] * free
@@ -604,7 +607,7 @@
         out_specs=[pl.BlockSpec(memory_space=pltpu.VMEM)] * len(outs),
         scratch_shapes=list(scratch),
         cost_estimate=pl.CostEstimate(flops=flops, bytes_accessed=1 << 20, transcendentals=0),
-        compiler_params=pltpu.CompilerParams(vmem_limit_bytes=56 << 20),
+        compiler_params=pltpu.CompilerParams(vmem_limit_bytes=grant << 20),
     )(*args)
 
 
@@ -636,17 +639,23 @@
     up_z3 = pairs(lambda x, z, y, c: (x, z + 1, y, c) if z == n_z - 2 else None)
     down_z3 = pairs(lambda x, z, y, c: (x, z - 1, y, c) if z == 1 else None)
 
+    up_z3_direct = pairs(lambda x, z, y, c: (x, n_z - 1, y, c) if z == n_z - 3 else None)
+    down_z3_direct = pairs(lambda x, z, y, c: (x, 0, y, c) if z == 2 else None)
+
     def move(value, perm):
         return lax.ppermute(value, axes, perm)
 
-    def gather(own, received):
-        slot = jnp.concatenate([own, received], axis=0)
+    def gather(slot, direct=False):
         r1 = move(slot, up_z)
         l1 = move(slot, down_z)
         r2 = move(r1, up_z2)
         l2 = move(l1, down_z2)
-        r3 = move(r2, up_z3)
-        l3 = move(l2, down_z3)
+        if direct:
+            r3 = move(r1, up_z3_direct)
+            l3 = move(l1, down_z3_direct)
+        else:
+            r3 = move(r2, up_z3)
+            l3 = move(l2, down_z3)
         return slot, r1, l1, r2, l2, r3, l3
 
     def shards(
@@ -700,13 +709,15 @@
                 result_switch_matrix,
                 attend_result_matrix,
             ),
+            grant=56,
         )
         spike_o, to_x, to_y, to_d = call(
             input_kernel,
             [((span, LANES), BF16)] + [((span, width + LANES), BF16)] * 3,
             (pos, spike_forget_logarithm, incoming_features),
-        )
-        attn = gather(own, move(send, over_y))
+            grant=56,
+        )
+        attn = gather(jnp.concatenate([own, move(send, over_y)], axis=0))
         from_x = move(to_x, over_x)
         from_y = move(to_y, over_y)
         from_d = move(to_d, over_d)
@@ -726,8 +737,10 @@
             return lax.dynamic_slice_in_dim(contract_matrix, index * ff, ff, 0)
 
         across = 2 * x + (1 - y)
-        up = gather(up_part(quarter), move(up_part(across), over_y))
-        down = gather(down_part(quarter), move(down_part(across), over_y))
+        up = gather(up_part(quarter))
+        up = up + gather(move(up_part(across), over_y))
+        down_own = gather(down_part(quarter), direct=True)
+        down_across = gather(move(down_part(across), over_y))
 
         def halves(blocks):
             mine = jnp.concatenate(blocks, axis=0)
@@ -784,6 +797,7 @@
                 pltpu.VMEM((tokens, LANES), BF16),
                 pltpu.SemaphoreType.DMA((48,)),
             ],
+            grant=56,
             flops=10**10,
             free=7,
         )
@@ -799,15 +813,14 @@
             (pos, mine, theirs, perceptron_scale.reshape(1, embed), taps_v, taps_g) + up,
             scratch=[pltpu.VMEM((embed, 2 * ff), BF16), pltpu.SemaphoreType.DMA((8,))],
             flops=10**10,
-            free=7,
+            free=14,
         )
         half = width // 2
-        slot_o, slot_r1, slot_l1, slot_r2, slot_l2, slot_r3, slot_l3 = down
         parts = []
-        for kernel, slots in (
-            (contract_kernel_one, (slot_o, slot_r2, slot_l2)),
-            (contract_kernel_two, (slot_r1, slot_l1, slot_r3, slot_l3)),
+        for kernel, places in (
+            (contract_kernel_one, (0, 3, 4)), (contract_kernel_two, (1, 2, 5, 6))
         ):
+            slots = tuple(group[place] for group in (down_own, down_across) for place in places)
             keep, other = call(
                 kernel,
                 [((tokens, half), BF16)] * 2,

time: 255 us -> 265 us (1.039)
  starting transfers between devices: 52.2 us -> 69 us
  Pallas kernels: 41.9 us -> 32.5 us
  waiting for transfers between devices: 145 us -> 149 us
  local copies, waits for them, and re-layouts: 9.54 us -> 5.55 us
    ppermute x41 -> x53, starting transfers between devices: 52.2 us -> 69 us  [move(): return lax.ppermute(value, axes, perm)]
    pallas_call x6, Pallas kernels: 41.9 us -> 32.5 us  [call(): pl.pallas_call(kernel, out_shape=[jax.ShapeDtypeStruct(*o) for o in outs]...]
    ppermute x41 -> x53, waiting for transfers between devices: 145 us -> 149 us  [move(): return lax.ppermute(value, axes, perm)]
  transfers between devices with their start and end apart: 41 -> 53, of which waited for: 20 -> 24; matrix products, arithmetic and copies ran while one was open for 4% -> 2% of each run, Pallas kernels for 7% -> 5%
where the time goes in v1:
time: 265 us; the launch traced here: 263 us
  waiting for transfers between devices  149 us (56%)
  starting transfers between devices  69 us (26%)
  Pallas kernels  32.5 us (12%)
  other arithmetic  5.9 us (2%)
  local copies, waits for them, and re-layouts  5.55 us (2%)
    ppermute x53, waiting for transfers between devices, move(): return lax.ppermute(value, axes, perm)  149 us
    ppermute x53, starting transfers between devices, move(): return lax.ppermute(value, axes, perm)  69 us
    pallas_call x6, Pallas kernels, call(): pl.pallas_call(kernel, out_shape=[jax.ShapeDtypeStruct(*o) for o in outs]...  32.5 us
  transfers between devices with their start and end apart: 53, of which 24 were waited for; matrix products, arithmetic and copies ran while one was open for 2% of the time, Pallas kernels for 5%

profile of v1, /device:TPU:0, one launch (start us, length us, event | category | flops | bytes accessed | tf_op | source)
XLA Modules:
  0.0 262.9 jit_solution(1115971506699075462)
XLA Ops:
  0.7 2.3 shard_map.164
  3.0 3.0 %collective-permute-start.4 = (bf16[1152,128]{1,0:T(8,128)(2,1)}, bf16[1152,128]{1,0:T(8,128)(2,1)S(1)}, u32[]{:S(2)}, u32[]{:S(2)}) collective-permute-start(bf16[1152,128]{1,0:T(8,128)(2,1)} %get-tuple-element.22), channel_id=1, source_target_pairs={{0,2},{1,3},{2,0},{3,1},{4,6},{5,7},{6,4},{7,5},{8,10},{9,11},{10,... | collective-permute-start | bytes 884744 | tf_op jit(solution)/shard_map/ppermute | solution.py:646
  6.0 2.9 %shard_map.163 = (bf16[192,128]{1,0:T(8,128)(2,1)}, bf16[192,1152]{1,0:T(8,128)(2,1)}, bf16[192,1152]{1,0:T(8,128)(2,1)}, bf16[192,1152]{1,0:T(8,128)(2,1)}) custom-call(s32[9]{0:T(128)} %stack.32.pos, f32[192,256]{1,0:T(8,128)} %spike.1, bf16[192,1024]{1,0:T(8,128)(2,1)} %feat.1), custom_call_target="tpu_custom_call" | custom-call | bytes 1048576 | tf_op jit(solution)/shard_map/pallas_call | solution.py:603
  15.3 4.6 %collective-permute-start.5 = (bf16[2304,128]{1,0:T(8,128)(2,1)S(1)}, bf16[2304,128]{1,0:T(8,128)(2,1)S(1)}, u32[]{:S(2)}, u32[]{:S(2)}) collective-permute-start(bf16[2304,128]{1,0:T(8,128)(2,1)S(1)} %constant_dynamic-update-slice_fusion.slot_o), channel_id=1, source_target_pairs={{0,4},{1,5},{2,6},{3,7},{4,8},{5,9},{6,10},{7,11},{8,12},{9,13},{1... | collective-permute-start | bytes 1769480 | tf_op jit(solution)/shard_map/ppermute | solution.py:646
  19.9 2.3 collective-permute-done.spike_x
  22.2 10.0 %collective-permute-done.1.spike_y = bf16[192,1152]{1,0:T(8,128)(2,1)S(1)} collective-permute-done((bf16[192,1152]{1,0:T(8,128)(2,1)}, bf16[192,1152]{1,0:T(8,128)(2,1)S(1)}, u32[]{:S(2)}, u32[]{:S(2)}) %collective-permute-start.1) | collective-permute-done | bytes 442400 | tf_op jit(solution)/shard_map/ppermute | solution.py:646
  35.2 15.6 %collective-permute-done.8.slot_l2 = bf16[2304,128]{1,0:T(8,128)(2,1)S(1)} collective-permute-done((bf16[2304,128]{1,0:T(8,128)(2,1)S(1)}, bf16[2304,128]{1,0:T(8,128)(2,1)S(1)}, u32[]{:S(2)}, u32[]{:S(2)}) %collective-permute-start.8) | collective-permute-done | bytes 589856 | tf_op jit(solution)/shard_map/ppermute | solution.py:646
  55.6 12.2 %collective-permute-done.10.slot_l3 = bf16[2304,128]{1,0:T(8,128)(2,1)} collective-permute-done((bf16[2304,128]{1,0:T(8,128)(2,1)S(1)}, bf16[2304,128]{1,0:T(8,128)(2,1)}, u32[]{:S(2)}, u32[]{:S(2)}) %collective-permute-start.10) | collective-permute-done | bytes 589856 | tf_op jit(solution)/shard_map/ppermute | solution.py:646
  67.8 16.9 %shard_map.165 = (bf16[768,1024]{1,0:T(8,128)(2,1)}, bf16[768,1024]{1,0:T(8,128)(2,1)}) custom-call(s32[9]{0:T(128)} %stack.32.pos, bf16[768,1024]{1,0:T(8,128)(2,1)} %copy-done.3, bf16[768,1024]{1,0:T(8,128)(2,1)} %collective-permute-done.3.theirs, bf16[1,2048]{1,0:T(2,128)(2,1)} %reshape.12.scale, f32[1,128]{1,0:T(1,128)} %maximum_bitcast_fusion.shift, ...), custom_call_target="tpu_custom_call" | custom-call | flops 10000000000 | bytes 1048576 | tf_op jit(solution)/shard_map/pallas_call | solution.py:603
  84.8 3.6 %collective-permute-done.11 = bf16[768,1024]{1,0:T(8,128)(2,1)S(1)} collective-permute-done((bf16[768,1024]{1,0:T(8,128)(2,1)}, bf16[768,1024]{1,0:T(8,128)(2,1)S(1)}, u32[]{:S(2)}, u32[]{:S(2)}) %collective-permute-start.11) | collective-permute-done | bytes 1572896 | tf_op jit(solution)/shard_map/ppermute | solution.py:646
  88.4 2.1 add_convert_fusion
  97.4 5.2 %collective-permute-done.12 = bf16[192,1024]{1,0:T(8,128)(2,1)S(1)} collective-permute-done((bf16[192,1024]{1,0:T(8,128)(2,1)S(1)}, bf16[192,1024]{1,0:T(8,128)(2,1)S(1)}, u32[]{:S(2)}, u32[]{:S(2)}) %collective-permute-start.12) | collective-permute-done | bytes 393248 | tf_op jit(solution)/shard_map/ppermute | solution.py:646
  103.9 8.7 %collective-permute-done.13 = bf16[192,1024]{1,0:T(8,128)(2,1)S(1)} collective-permute-done((bf16[192,1024]{1,0:T(8,128)(2,1)S(1)}, bf16[192,1024]{1,0:T(8,128)(2,1)S(1)}, u32[]{:S(2)}, u32[]{:S(2)}) %collective-permute-start.13) | collective-permute-done | bytes 393248 | tf_op jit(solution)/shard_map/ppermute | solution.py:646
  116.0 12.4 %collective-permute-done.36.refs_3_ = bf16[512,256]{1,0:T(8,128)(2,1)S(1)} collective-permute-done((bf16[512,256]{1,0:T(8,128)(2,1)S(1)}, bf16[512,256]{1,0:T(8,128)(2,1)S(1)}, u32[]{:S(2)}, u32[]{:S(2)}) %collective-permute-start.36) | collective-permute-done | bytes 262176 | tf_op jit(solution)/shard_map/ppermute | solution.py:646
  133.2 4.6 %collective-permute-start.37 = (bf16[512,256]{1,0:T(8,128)(2,1)S(1)}, bf16[512,256]{1,0:T(8,128)(2,1)S(1)}, u32[]{:S(2)}, u32[]{:S(2)}) collective-permute-start(bf16[512,256]{1,0:T(8,128)(2,1)S(1)} %collective-permute-done.36.refs_3_), channel_id=1, source_target_pairs={{0,4},{1,5},{2,6},{3,7},{4,8},{5,9},{6,10},{7,11},{8,12},{9,13},{1... | collective-permute-start | bytes 786440 | tf_op jit(solution)/shard_map/ppermute | solution.py:646
  137.7 2.6 collective-permute-done.15
  141.6 4.5 %collective-permute-done.16 = bf16[192,1024]{1,0:T(8,128)(2,1)S(1)} collective-permute-done((bf16[192,1024]{1,0:T(8,128)(2,1)S(1)}, bf16[192,1024]{1,0:T(8,128)(2,1)S(1)}, u32[]{:S(2)}, u32[]{:S(2)}) %collective-permute-start.16) | collective-permute-done | bytes 393248 | tf_op jit(solution)/shard_map/ppermute | solution.py:646
  150.0 2.4 collective-permute-done.39.refs_5_
  154.3 13.9 %collective-permute-done.40.refs_5_ = bf16[512,256]{1,0:T(8,128)(2,1)S(1)} collective-permute-done((bf16[512,256]{1,0:T(8,128)(2,1)S(1)}, bf16[512,256]{1,0:T(8,128)(2,1)S(1)}, u32[]{:S(2)}, u32[]{:S(2)}) %collective-permute-start.40) | collective-permute-done | bytes 262176 | tf_op jit(solution)/shard_map/ppermute | solution.py:646
  172.2 12.7 %collective-permute-done.22.refs_4_ = bf16[256,1024]{1,0:T(8,128)(2,1)S(1)} collective-permute-done((bf16[256,1024]{1,0:T(8,128)(2,1)S(1)}, bf16[256,1024]{1,0:T(8,128)(2,1)S(1)}, u32[]{:S(2)}, u32[]{:S(2)}) %collective-permute-start.22) | collective-permute-done | bytes 524320 | tf_op jit(solution)/shard_map/ppermute | solution.py:646
  187.1 9.1 %collective-permute-done.29.refs_11_ = bf16[256,1024]{1,0:T(8,128)(2,1)S(1)} collective-permute-done((bf16[256,1024]{1,0:T(8,128)(2,1)S(1)}, bf16[256,1024]{1,0:T(8,128)(2,1)S(1)}, u32[]{:S(2)}, u32[]{:S(2)}) %collective-permute-start.29) | collective-permute-done | bytes 524320 | tf_op jit(solution)/shard_map/ppermute | solution.py:646
  198.8 8.5 %collective-permute-done.24.refs_6_ = bf16[256,1024]{1,0:T(8,128)(2,1)S(1)} collective-permute-done((bf16[256,1024]{1,0:T(8,128)(2,1)S(1)}, bf16[256,1024]{1,0:T(8,128)(2,1)S(1)}, u32[]{:S(2)}, u32[]{:S(2)}) %collective-permute-start.24) | collective-permute-done | bytes 524320 | tf_op jit(solution)/shard_map/ppermute | solution.py:646
  209.3 6.5 %collective-permute-done.31.refs_13_ = bf16[256,1024]{1,0:T(8,128)(2,1)S(1)} collective-permute-done((bf16[256,1024]{1,0:T(8,128)(2,1)S(1)}, bf16[256,1024]{1,0:T(8,128)(2,1)S(1)}, u32[]{:S(2)}, u32[]{:S(2)}) %collective-permute-start.31) | collective-permute-done | bytes 524320 | tf_op jit(solution)/shard_map/ppermute | solution.py:646
  217.9 7.0 %shard_map.166.hidden = bf16[768,512]{1,0:T(8,128)(2,1)S(1)} custom-call(s32[9]{0:T(128)S(1)} %copy-done.1, bf16[768,1024]{1,0:T(8,128)(2,1)S(1)} %pad_maximum_fusion.1.mine, bf16[768,1024]{1,0:T(8,128)(2,1)S(1)} %collective-permute-done.18.theirs, bf16[1,2048]{1,0:T(2,128)(2,1)S(1)} %reshape.15.scale, bf16[3,512]{1,0:T(4,128)(2,1)S(1)} %get-tuple-element.50.taps_v, ...), custom_call_target="tpu_custom_call" | custom-call | flops 10000000000 | bytes 1048576 | tf_op jit(solution)/shard_map/pallas_call | solution.py:603
  227.0 4.9 %collective-permute-done.48.refs_7_ = bf16[512,256]{1,0:T(8,128)(2,1)S(1)} collective-permute-done((bf16[512,256]{1,0:T(8,128)(2,1)S(1)}, bf16[512,256]{1,0:T(8,128)(2,1)S(1)}, u32[]{:S(2)}, u32[]{:S(2)}) %collective-permute-start.48) | collective-permute-done | bytes 262176 | tf_op jit(solution)/shard_map/ppermute | solution.py:646
  231.9 1.7 shard_map.168
  237.3 3.9 %collective-permute-start.50 = (bf16[192,512]{1,0:T(8,128)(2,1)S(1)}, bf16[192,512]{1,0:T(8,128)(2,1)S(1)}, u32[]{:S(2)}, u32[]{:S(2)}) collective-permute-start(bf16[192,512]{1,0:T(8,128)(2,1)S(1)} %get-tuple-element.41), channel_id=1, source_target_pairs={{0,16},{1,17},{2,18},{3,19},{4,20},{5,21},{6,22},{7,23},{8,24},{9,... | collective-permute-start | bytes 589832 | tf_op jit(solution)/shard_map/ppermute | solution.py:646
  243.8 1.9 collective-permute-start.42
  247.3 2.7 %collective-permute-start.44 = (bf16[192,512]{1,0:T(8,128)(2,1)S(1)}, bf16[192,512]{1,0:T(8,128)(2,1)}, u32[]{:S(2)}, u32[]{:S(2)}) collective-permute-start(bf16[192,512]{1,0:T(8,128)(2,1)S(1)} %get-tuple-element.45), channel_id=1, source_target_pairs={{0,18},{1,19},{2,16},{3,17},{4,22},{5,23},{6,20},{7,21},{8,26},{9,... | collective-permute-start | bytes 589832 | tf_op jit(solution)/shard_map/ppermute | solution.py:646
  250.0 3.0 %collective-permute-done.51 = bf16[192,512]{1,0:T(8,128)(2,1)S(1)} collective-permute-done((bf16[192,512]{1,0:T(8,128)(2,1)S(1)}, bf16[192,512]{1,0:T(8,128)(2,1)S(1)}, u32[]{:S(2)}, u32[]{:S(2)}) %collective-permute-start.51) | collective-permute-done | bytes 196640 | tf_op jit(solution)/shard_map/ppermute | solution.py:646
  253.0 2.5 collective-permute-done.42
  255.5 5.4 %collective-permute-done.43 = bf16[192,512]{1,0:T(8,128)(2,1)S(1)} collective-permute-done((bf16[192,512]{1,0:T(8,128)(2,1)}, bf16[192,512]{1,0:T(8,128)(2,1)S(1)}, u32[]{:S(2)}, u32[]{:S(2)}) %collective-permute-start.43) | collective-permute-done | bytes 196640 | tf_op jit(solution)/shard_map/ppermute | solution.py:646
  (144 shorter events, 62.7 us)
Async XLA Ops:
  10.4 21.8 %collective-permute-start.1 = (bf16[192,1152]{1,0:T(8,128)(2,1)}, bf16[192,1152]{1,0:T(8,128)(2,1)S(1)}, u32[]{:S(2)}, u32[]{:S(2)}) collective-permute-start(bf16[192,1152]{1,0:T(8,128)(2,1)} %get-tuple-element.18), channel_id=1, source_target_pairs={{0,2},{1,3},{2,0},{3,1},{4,6},{5,7},{6,4},{7,5},{8,10},{9,11},{10,... | collective-permute-start | bytes 1327112 | tf_op jit(solution)/shard_map/ppermute | solution.py:646
  10.9 21.3 %collective-permute-start.2 = (bf16[192,1152]{1,0:T(8,128)(2,1)}, bf16[192,1152]{1,0:T(8,128)(2,1)S(1)}, u32[]{:S(2)}, u32[]{:S(2)}) collective-permute-start(bf16[192,1152]{1,0:T(8,128)(2,1)} %get-tuple-element.19), channel_id=1, source_target_pairs={{0,18},{1,19},{2,16},{3,17},{4,22},{5,23},{6,20},{7,21},{8,26},{9,... | collective-permute-start | bytes 1327112 | tf_op jit(solution)/shard_map/ppermute | solution.py:646
  14.0 19.1 %collective-permute-start.6 = (bf16[2304,128]{1,0:T(8,128)(2,1)S(1)}, bf16[2304,128]{1,0:T(8,128)(2,1)S(1)}, u32[]{:S(2)}, u32[]{:S(2)}) collective-permute-start(bf16[2304,128]{1,0:T(8,128)(2,1)S(1)} %constant_dynamic-update-slice_fusion.slot_o), channel_id=1, source_target_pairs={{4,0},{5,1},{6,2},{7,3},{8,4},{9,5},{10,6},{11,7},{12,8},{13,9},{1... | collective-permute-start | bytes 1769480 | tf_op jit(solution)/shard_map/ppermute | solution.py:646
  15.3 19.1 %collective-permute-start.5 = (bf16[2304,128]{1,0:T(8,128)(2,1)S(1)}, bf16[2304,128]{1,0:T(8,128)(2,1)S(1)}, u32[]{:S(2)}, u32[]{:S(2)}) collective-permute-start(bf16[2304,128]{1,0:T(8,128)(2,1)S(1)} %constant_dynamic-update-slice_fusion.slot_o), channel_id=1, source_target_pairs={{0,4},{1,5},{2,6},{3,7},{4,8},{5,9},{6,10},{7,11},{8,12},{9,13},{1... | collective-permute-start | bytes 1769480 | tf_op jit(solution)/shard_map/ppermute | solution.py:646
  33.1 22.4 %collective-permute-start.3 = (bf16[768,1024]{1,0:T(8,128)(2,1)S(1)}, bf16[768,1024]{1,0:T(8,128)(2,1)}, u32[]{:S(2)}, u32[]{:S(2)}) collective-permute-start(bf16[768,1024]{1,0:T(8,128)(2,1)S(1)} %pad_maximum_fusion.mine), channel_id=1, source_target_pairs={{0,1},{1,0},{2,3},{3,2},{4,5},{5,4},{6,7},{7,6},{8,9},{9,8},{10,11... | collective-permute-start | bytes 4718600 | tf_op jit(solution)/shard_map/ppermute | solution.py:646
  33.2 17.7 %collective-permute-start.8 = (bf16[2304,128]{1,0:T(8,128)(2,1)S(1)}, bf16[2304,128]{1,0:T(8,128)(2,1)S(1)}, u32[]{:S(2)}, u32[]{:S(2)}) collective-permute-start(bf16[2304,128]{1,0:T(8,128)(2,1)S(1)} %collective-permute-done.6.slot_l1), channel_id=1, source_target_pairs={{4,0},{5,1},{6,2},{7,3},{8,4},{9,5},{10,6},{11,7},{20,16},{21,17},... | collective-permute-start | bytes 1769480 | tf_op jit(solution)/shard_map/ppermute | solution.py:646
  34.5 17.6 %collective-permute-start.7 = (bf16[2304,128]{1,0:T(8,128)(2,1)S(1)}, bf16[2304,128]{1,0:T(8,128)(2,1)S(1)}, u32[]{:S(2)}, u32[]{:S(2)}) collective-permute-start(bf16[2304,128]{1,0:T(8,128)(2,1)S(1)} %collective-permute-done.5.slot_r1), channel_id=1, source_target_pairs={{4,8},{5,9},{6,10},{7,11},{8,12},{9,13},{10,14},{11,15},{20,24},{2... | collective-permute-start | bytes 1769480 | tf_op jit(solution)/shard_map/ppermute | solution.py:646
  50.8 16.9 %collective-permute-start.10 = (bf16[2304,128]{1,0:T(8,128)(2,1)S(1)}, bf16[2304,128]{1,0:T(8,128)(2,1)}, u32[]{:S(2)}, u32[]{:S(2)}) collective-permute-start(bf16[2304,128]{1,0:T(8,128)(2,1)S(1)} %collective-permute-done.8.slot_l2), channel_id=1, source_target_pairs={{4,0},{5,1},{6,2},{7,3},{20,16},{21,17},{22,18},{23,19}} | collective-permute-start | bytes 1769480 | tf_op jit(solution)/shard_map/ppermute | solution.py:646
  92.2 20.4 %collective-permute-start.13 = (bf16[192,1024]{1,0:T(8,128)(2,1)S(1)}, bf16[192,1024]{1,0:T(8,128)(2,1)S(1)}, u32[]{:S(2)}, u32[]{:S(2)}) collective-permute-start(bf16[192,1024]{1,0:T(8,128)(2,1)S(1)} %get-tuple-element.34), channel_id=1, source_target_pairs={{0,2},{1,3},{2,0},{3,1},{4,6},{5,7},{6,4},{7,5},{8,10},{9,11},{10,... | collective-permute-start | bytes 1179656 | tf_op jit(solution)/shard_map/ppermute | solution.py:646
  93.7 20.3 %collective-permute-start.14 = (bf16[192,1024]{1,0:T(8,128)(2,1)S(1)}, bf16[192,1024]{1,0:T(8,128)(2,1)S(1)}, u32[]{:S(2)}, u32[]{:S(2)}) collective-permute-start(bf16[192,1024]{1,0:T(8,128)(2,1)S(1)} %get-tuple-element.33), channel_id=1, source_target_pairs={{0,18},{1,19},{2,16},{3,17},{4,22},{5,23},{6,20},{7,21},{8,26},{9,... | collective-permute-start | bytes 1179656 | tf_op jit(solution)/shard_map/ppermute | solution.py:646
  94.3 37.6 %collective-permute-start.25 = (bf16[256,1024]{1,0:T(8,128)(2,1)S(1)}, bf16[256,1024]{1,0:T(8,128)(2,1)S(1)}, u32[]{:S(2)}, u32[]{:S(2)}) collective-permute-start(bf16[256,1024]{1,0:T(8,128)(2,1)S(1)} %pad_maximum_fusion.3), channel_id=1, source_target_pairs={{0,2},{1,3},{2,0},{3,1},{4,6},{5,7},{6,4},{7,5},{8,10},{9,11},{10,... | collective-permute-start | bytes 1572872 | tf_op jit(solution)/shard_map/ppermute | solution.py:646
  96.0 32.8 %collective-permute-start.32 = (bf16[512,256]{1,0:T(8,128)(2,1)S(1)}, bf16[512,256]{1,0:T(8,128)(2,1)S(1)}, u32[]{:S(2)}, u32[]{:S(2)}) collective-permute-start(bf16[512,256]{1,0:T(8,128)(2,1)S(1)} %get-tuple-element.36.refs_0_), channel_id=1, source_target_pairs={{0,4},{1,5},{2,6},{3,7},{4,8},{5,9},{6,10},{7,11},{8,12},{9,13},{1... | collective-permute-start | bytes 786440 | tf_op jit(solution)/shard_map/ppermute | solution.py:646
  102.6 27.8 %collective-permute-start.34 = (bf16[512,256]{1,0:T(8,128)(2,1)S(1)}, bf16[512,256]{1,0:T(8,128)(2,1)S(1)}, u32[]{:S(2)}, u32[]{:S(2)}) collective-permute-start(bf16[512,256]{1,0:T(8,128)(2,1)S(1)} %get-tuple-element.36.refs_0_), channel_id=1, source_target_pairs={{4,0},{5,1},{6,2},{7,3},{8,4},{9,5},{10,6},{11,7},{12,8},{13,9},{1... | collective-permute-start | bytes 786440 | tf_op jit(solution)/shard_map/ppermute | solution.py:646
  112.6 20.5 %collective-permute-start.19 = (bf16[256,1024]{1,0:T(8,128)(2,1)S(1)}, bf16[256,1024]{1,0:T(8,128)(2,1)S(1)}, u32[]{:S(2)}, u32[]{:S(2)}) collective-permute-start(bf16[256,1024]{1,0:T(8,128)(2,1)S(1)} %pad_maximum_fusion.2.refs_0_), channel_id=1, source_target_pairs={{0,4},{1,5},{2,6},{3,7},{4,8},{5,9},{6,10},{7,11},{8,12},{9,13},{1... | collective-permute-start | bytes 1572872 | tf_op jit(solution)/shard_map/ppermute | solution.py:646
  128.8 17.3 %collective-permute-start.16 = (bf16[192,1024]{1,0:T(8,128)(2,1)S(1)}, bf16[192,1024]{1,0:T(8,128)(2,1)S(1)}, u32[]{:S(2)}, u32[]{:S(2)}) collective-permute-start(bf16[192,1024]{1,0:T(8,128)(2,1)S(1)} %add_convert_fusion.3), channel_id=1, source_target_pairs={{0,2},{1,3},{2,0},{3,1},{4,6},{5,7},{6,4},{7,5},{8,10},{9,11},{10,... | collective-permute-start | bytes 1179656 | tf_op jit(solution)/shard_map/ppermute | solution.py:646
  130.4 17.3 %collective-permute-start.17 = (bf16[192,1024]{1,0:T(8,128)(2,1)S(1)}, bf16[192,1024]{1,0:T(8,128)(2,1)S(1)}, u32[]{:S(2)}, u32[]{:S(2)}) collective-permute-start(bf16[192,1024]{1,0:T(8,128)(2,1)S(1)} %add_convert_fusion.3), channel_id=1, source_target_pairs={{0,18},{1,19},{2,16},{3,17},{4,22},{5,23},{6,20},{7,21},{8,26},{9,... | collective-permute-start | bytes 1179656 | tf_op jit(solution)/shard_map/ppermute | solution.py:646
  131.9 17.3 %collective-permute-start.20 = (bf16[256,1024]{1,0:T(8,128)(2,1)S(1)}, bf16[256,1024]{1,0:T(8,128)(2,1)S(1)}, u32[]{:S(2)}, u32[]{:S(2)}) collective-permute-start(bf16[256,1024]{1,0:T(8,128)(2,1)S(1)} %pad_maximum_fusion.2.refs_0_), channel_id=1, source_target_pairs={{4,0},{5,1},{6,2},{7,3},{8,4},{9,5},{10,6},{11,7},{12,8},{13,9},{1... | collective-permute-start | bytes 1572872 | tf_op jit(solution)/shard_map/ppermute | solution.py:646
  133.2 16.1 %collective-permute-start.37 = (bf16[512,256]{1,0:T(8,128)(2,1)S(1)}, bf16[512,256]{1,0:T(8,128)(2,1)S(1)}, u32[]{:S(2)}, u32[]{:S(2)}) collective-permute-start(bf16[512,256]{1,0:T(8,128)(2,1)S(1)} %collective-permute-done.36.refs_3_), channel_id=1, source_target_pairs={{0,4},{1,5},{2,6},{3,7},{4,8},{5,9},{6,10},{7,11},{8,12},{9,13},{1... | collective-permute-start | bytes 786440 | tf_op jit(solution)/shard_map/ppermute | solution.py:646
  146.1 23.4 %collective-permute-start.26 = (bf16[256,1024]{1,0:T(8,128)(2,1)S(1)}, bf16[256,1024]{1,0:T(8,128)(2,1)S(1)}, u32[]{:S(2)}, u32[]{:S(2)}) collective-permute-start(bf16[256,1024]{1,0:T(8,128)(2,1)S(1)} %collective-permute-done.25.refs_7_), channel_id=1, source_target_pairs={{0,4},{1,5},{2,6},{3,7},{4,8},{5,9},{6,10},{7,11},{8,12},{9,13},{1... | collective-permute-start | bytes 1572872 | tf_op jit(solution)/shard_map/ppermute | solution.py:646
  147.8 22.4 %collective-permute-start.27 = (bf16[256,1024]{1,0:T(8,128)(2,1)S(1)}, bf16[256,1024]{1,0:T(8,128)(2,1)S(1)}, u32[]{:S(2)}, u32[]{:S(2)}) collective-permute-start(bf16[256,1024]{1,0:T(8,128)(2,1)S(1)} %collective-permute-done.25.refs_7_), channel_id=1, source_target_pairs={{4,0},{5,1},{6,2},{7,3},{8,4},{9,5},{10,6},{11,7},{12,8},{13,9},{1... | collective-permute-start | bytes 1572872 | tf_op jit(solution)/shard_map/ppermute | solution.py:646
  149.2 67.4 %collective-permute-start.18 = (bf16[768,1024]{1,0:T(8,128)(2,1)S(1)}, bf16[768,1024]{1,0:T(8,128)(2,1)S(1)}, u32[]{:S(2)}, u32[]{:S(2)}) collective-permute-start(bf16[768,1024]{1,0:T(8,128)(2,1)S(1)} %pad_maximum_fusion.1.mine), channel_id=1, source_target_pairs={{0,1},{1,0},{2,3},{3,2},{4,5},{5,4},{6,7},{7,6},{8,9},{9,8},{10,11... | collective-permute-start | bytes 4718600 | tf_op jit(solution)/shard_map/ppermute | solution.py:646
  153.6 17.9 %collective-permute-start.21 = (bf16[256,1024]{1,0:T(8,128)(2,1)S(1)}, bf16[256,1024]{1,0:T(8,128)(2,1)S(1)}, u32[]{:S(2)}, u32[]{:S(2)}) collective-permute-start(bf16[256,1024]{1,0:T(8,128)(2,1)S(1)} %collective-permute-done.19.refs_1_), channel_id=1, source_target_pairs={{4,8},{5,9},{6,10},{7,11},{8,12},{9,13},{10,14},{11,15},{20,24},{2... | collective-permute-start | bytes 1572872 | tf_op jit(solution)/shard_map/ppermute | solution.py:646
  168.2 16.7 %collective-permute-start.22 = (bf16[256,1024]{1,0:T(8,128)(2,1)S(1)}, bf16[256,1024]{1,0:T(8,128)(2,1)S(1)}, u32[]{:S(2)}, u32[]{:S(2)}) collective-permute-start(bf16[256,1024]{1,0:T(8,128)(2,1)S(1)} %collective-permute-done.20.refs_2_), channel_id=1, source_target_pairs={{4,0},{5,1},{6,2},{7,3},{8,4},{9,5},{10,6},{11,7},{20,16},{21,17},... | collective-permute-start | bytes 1572872 | tf_op jit(solution)/shard_map/ppermute | solution.py:646
  169.5 16.9 %collective-permute-start.28 = (bf16[256,1024]{1,0:T(8,128)(2,1)S(1)}, bf16[256,1024]{1,0:T(8,128)(2,1)S(1)}, u32[]{:S(2)}, u32[]{:S(2)}) collective-permute-start(bf16[256,1024]{1,0:T(8,128)(2,1)S(1)} %collective-permute-done.26.refs_8_), channel_id=1, source_target_pairs={{4,8},{5,9},{6,10},{7,11},{8,12},{9,13},{10,14},{11,15},{20,24},{2... | collective-permute-start | bytes 1572872 | tf_op jit(solution)/shard_map/ppermute | solution.py:646
  170.2 25.9 %collective-permute-start.29 = (bf16[256,1024]{1,0:T(8,128)(2,1)S(1)}, bf16[256,1024]{1,0:T(8,128)(2,1)S(1)}, u32[]{:S(2)}, u32[]{:S(2)}) collective-permute-start(bf16[256,1024]{1,0:T(8,128)(2,1)S(1)} %collective-permute-done.27.refs_9_), channel_id=1, source_target_pairs={{4,0},{5,1},{6,2},{7,3},{8,4},{9,5},{10,6},{11,7},{20,16},{21,17},... | collective-permute-start | bytes 1572872 | tf_op jit(solution)/shard_map/ppermute | solution.py:646
  171.5 26.6 %collective-permute-start.23 = (bf16[256,1024]{1,0:T(8,128)(2,1)S(1)}, bf16[256,1024]{1,0:T(8,128)(2,1)S(1)}, u32[]{:S(2)}, u32[]{:S(2)}) collective-permute-start(bf16[256,1024]{1,0:T(8,128)(2,1)S(1)} %collective-permute-done.21.refs_3_), channel_id=1, source_target_pairs={{8,12},{9,13},{10,14},{11,15},{24,28},{25,29},{26,30},{27,31}} | collective-permute-start | bytes 1572872 | tf_op jit(solution)/shard_map/ppermute | solution.py:646
  184.9 22.5 %collective-permute-start.24 = (bf16[256,1024]{1,0:T(8,128)(2,1)S(1)}, bf16[256,1024]{1,0:T(8,128)(2,1)S(1)}, u32[]{:S(2)}, u32[]{:S(2)}) collective-permute-start(bf16[256,1024]{1,0:T(8,128)(2,1)S(1)} %collective-permute-done.22.refs_4_), channel_id=1, source_target_pairs={{4,0},{5,1},{6,2},{7,3},{20,16},{21,17},{22,18},{23,19}} | collective-permute-start | bytes 1572872 | tf_op jit(solution)/shard_map/ppermute | solution.py:646
  186.4 21.7 %collective-permute-start.30 = (bf16[256,1024]{1,0:T(8,128)(2,1)S(1)}, bf16[256,1024]{1,0:T(8,128)(2,1)S(1)}, u32[]{:S(2)}, u32[]{:S(2)}) collective-permute-start(bf16[256,1024]{1,0:T(8,128)(2,1)S(1)} %collective-permute-done.28.refs_10_), channel_id=1, source_target_pairs={{8,12},{9,13},{10,14},{11,15},{24,28},{25,29},{26,30},{27,31}} | collective-permute-start | bytes 1572872 | tf_op jit(solution)/shard_map/ppermute | solution.py:646
  196.1 19.8 %collective-permute-start.31 = (bf16[256,1024]{1,0:T(8,128)(2,1)S(1)}, bf16[256,1024]{1,0:T(8,128)(2,1)S(1)}, u32[]{:S(2)}, u32[]{:S(2)}) collective-permute-start(bf16[256,1024]{1,0:T(8,128)(2,1)S(1)} %collective-permute-done.29.refs_11_), channel_id=1, source_target_pairs={{4,0},{5,1},{6,2},{7,3},{20,16},{21,17},{22,18},{23,19}} | collective-permute-start | bytes 1572872 | tf_op jit(solution)/shard_map/ppermute | solution.py:646
  198.2 26.7 %collective-permute-start.45 = (bf16[512,256]{1,0:T(8,128)(2,1)S(1)}, bf16[512,256]{1,0:T(8,128)(2,1)S(1)}, u32[]{:S(2)}, u32[]{:S(2)}) collective-permute-start(bf16[512,256]{1,0:T(8,128)(2,1)S(1)} %collective-permute-done.32.refs_0_), channel_id=1, source_target_pairs={{4,12},{5,13},{6,14},{7,15},{20,28},{21,29},{22,30},{23,31}} | collective-permute-start | bytes 786440 | tf_op jit(solution)/shard_map/ppermute | solution.py:646
  207.4 26.3 %collective-permute-start.33 = (bf16[512,256]{1,0:T(8,128)(2,1)S(1)}, bf16[512,256]{1,0:T(8,128)(2,1)S(1)}, u32[]{:S(2)}, u32[]{:S(2)}) collective-permute-start(bf16[512,256]{1,0:T(8,128)(2,1)S(1)} %collective-permute-done.32.refs_0_), channel_id=1, source_target_pairs={{4,8},{5,9},{6,10},{7,11},{8,12},{9,13},{10,14},{11,15},{20,24},{2... | collective-permute-start | bytes 786440 | tf_op jit(solution)/shard_map/ppermute | solution.py:646
  208.0 19.0 %collective-permute-start.46 = (bf16[512,256]{1,0:T(8,128)(2,1)S(1)}, bf16[512,256]{1,0:T(8,128)(2,1)S(1)}, u32[]{:S(2)}, u32[]{:S(2)}) collective-permute-start(bf16[512,256]{1,0:T(8,128)(2,1)S(1)} %collective-permute-done.34.refs_1_), channel_id=1, source_target_pairs={{8,0},{9,1},{10,2},{11,3},{24,16},{25,17},{26,18},{27,19}} | collective-permute-start | bytes 786440 | tf_op jit(solution)/shard_map/ppermute | solution.py:646
  (39 other events, 658.0 us)

commit v2 on v1

--- a/solution.py
+++ b/solution.py
@@ -357,6 +357,8 @@
         >= lax.broadcasted_iota(jnp.int32, (span, span), 1)
     ).astype(BF16)
     heads = LANES // HEAD_K
+    key_heads = lax.broadcasted_iota(jnp.int32, (1, LANES), 1) // HEAD_K
+    value_heads = lax.broadcasted_iota(jnp.int32, (1, 2 * LANES), 1) // HEAD_V
 
     def split_dot(a, value):
         one = value.astype(BF16)
@@ -426,25 +428,27 @@
             k_all = jnp.concatenate(k_parts, axis=0) if blocks > 1 else k_parts[0]
             v_all = (jnp.concatenate(v_parts, axis=0) if blocks > 1 else v_parts[0]).astype(BF16)
             n_q, n_k = q_all.shape[0], k_all.shape[0]
-            q_lane = lax.broadcasted_iota(jnp.int32, (n_q, LANES), 1) // HEAD_K
             q_heads = jnp.concatenate(
-                [jnp.where(q_lane == h, q_all, 0.0) for h in range(heads)], axis=0
-            ).astype(BF16)
+                [jnp.where(key_heads == h, q_all, 0.0).astype(BF16) for h in range(heads)],
+                axis=0,
+            )
             scores = lax.dot_general(
                 q_heads, k_all.astype(BF16), (((1,), (1,)), ((), ())), preferred_element_type=F32
             )
             if blocks > 1:
-                q_block = (
-                    lax.rem(lax.broadcasted_iota(jnp.int32, (heads * n_q, n_k), 0), n_q)
-                    // second_rows
+                shift_by = size.bit_length() - 1
+                q_block = lax.shift_right_logical(
+                    lax.broadcasted_iota(jnp.int32, (n_q, n_k), 0), shift_by
                 )
-                k_block = lax.broadcasted_iota(jnp.int32, (heads * n_q, n_k), 1) // size
-                scores = jnp.where(q_block == k_block, scores, 0.0)
+                k_block = lax.shift_right_logical(
+                    lax.broadcasted_iota(jnp.int32, (n_q, n_k), 1), shift_by
+                )
+                same_block = (q_block == k_block).astype(F32)
+                scores = scores * jnp.concatenate([same_block] * heads, axis=0)
             wide = dot(scores.astype(BF16), v_all)
-            wide_lane = lax.broadcasted_iota(jnp.int32, (n_q, 2 * LANES), 1) // HEAD_V
             total = wide[0:n_q]
             for h in range(1, heads):
-                total = jnp.where(wide_lane == h, wide[h * n_q : (h + 1) * n_q], total)
+                total = jnp.where(value_heads == h, wide[h * n_q : (h + 1) * n_q], total)
             zeros = jnp.zeros((size, 2 * LANES), F32)
             full = []
             for i in range(blocks):
@@ -546,60 +550,32 @@
     lax.fori_loop(0, 4, sequence, 0)
 
 
-def contract_pair(pos, hidden, shards, keep, send, weights, sems):
-    y = pos[7]
+def contract_kernel(
+    pos, hidden, slot_o, slot_r1, slot_l1, slot_r2, slot_l2, slot_r3, slot_l3,
+    keep, send, weights, sems,
+):
+    core = pos[5]
     width = weights.shape[3]
+    slots = (slot_o, slot_r1, slot_l1, slot_r2, slot_l2, slot_r3, slot_l3)
     waits = []
-    for j, blocks in enumerate(shards):
-        for index, (where, choices) in enumerate(blocks):
-            dst = weights.at[where, y if j == 0 else 1 - y]
-            sem = sems.at[index * 2 + j]
-            copy_from(choices, sem, dst, lambda ref: ref)
-            waits.append((choices[0][1], dst, sem))
+    for index, (zi, choices) in enumerate(blocks_of(pos, slots)):
+        dst = weights.at[jnp.where((zi // 2) == core, 0, 1), lax.rem(zi, 2)]
+        sem = sems.at[index]
+        copy_from(choices, sem, dst, lambda ref: ref)
+        waits.append((slot_o, dst, sem))
     for source, dst, sem in waits:
         pltpu.make_async_copy(source, dst, sem).wait()
     for index, out in ((1, send), (0, keep)):
-        for side in range(2):
-            out[:, side * width : (side + 1) * width] = dot(
-                hidden[...], weights[index, side]
+        for low in range(2):
+            out[:, low * width : (low + 1) * width] = dot(
+                hidden[...], weights[index, low]
             ).astype(BF16)
 
 
-def contract_kernel_one(pos, hidden, *refs):
-    z = pos[6]
-    same = jnp.where((z // 2) == pos[5], 0, 1)
-    low = z < 2
-
-    def blocks(slot_o, slot_r2, slot_l2):
-        return (
-            (same, ((None, slot_o),)),
-            (1 - same, ((low, slot_l2), (jnp.logical_not(low), slot_r2))),
-        )
-
-    contract_pair(pos, hidden, (blocks(*refs[0:3]), blocks(*refs[3:6])), *refs[6:])
-
-
-def contract_kernel_two(pos, hidden, *refs):
-    z, last = pos[6], pos[8]
-    same = jnp.where((z // 2) == pos[5], 0, 1)
-    even = lax.rem(z, 2) == 0
-
-    def blocks(slot_r1, slot_l1, slot_r3, slot_l3):
-        return (
-            (same, ((even, slot_l1), (jnp.logical_not(even), slot_r1))),
-            (
-                1 - same,
-                ((z == 0, slot_l3), (z == 1, slot_l1), (z == 2, slot_r1), (z == last, slot_r3)),
-            ),
-        )
-
-    contract_pair(pos, hidden, (blocks(*refs[0:4]), blocks(*refs[4:8])), *refs[8:])
-
-
-def call(kernel, outs, args, scratch=(), flops=0, free=0, grant=24):
+def call(kernel, outs, args, scratch=(), flops=0, free=0, grant=24, fixed=False):
     in_specs = [pl.BlockSpec(memory_space=pltpu.SMEM)]
     in_specs += [pl.BlockSpec(memory_space=pltpu.VMEM)] * (len(args) - 1 - free)
-    in_specs += [pl.BlockSpec(memory_space=pl.ANY)] * free
+    in_specs += [pl.BlockSpec(memory_space=pltpu.HBM if fixed else pl.ANY)] * free
     return pl.pallas_call(
         kernel,
         out_shape=[jax.ShapeDtypeStruct(*o) for o in outs],
@@ -739,8 +715,9 @@
         across = 2 * x + (1 - y)
         up = gather(up_part(quarter))
         up = up + gather(move(up_part(across), over_y))
-        down_own = gather(down_part(quarter), direct=True)
-        down_across = gather(move(down_part(across), over_y))
+        kept, received = down_part(quarter), move(down_part(across), over_y)
+        down_own = gather(jnp.where(y == 0, kept, received), direct=True)
+        down_across = gather(jnp.where(y == 0, received, kept), direct=True)
 
         def halves(blocks):
             mine = jnp.concatenate(blocks, axis=0)
@@ -768,6 +745,9 @@
         shift = lax.dynamic_slice_in_dim(forgetting_shift, quarter * key_w, key_w, 0)
         shift = jnp.concatenate([shift, shift]).reshape(1, LANES)
         unit = lax.dynamic_slice_in_dim(attend_unit_scale, quarter * val_w, val_w, 0)
+        unit = unit.reshape(1, val_w)
+        before = attend_prenormal_scale.reshape(1, embed)
+        after = perceptron_scale.reshape(1, embed)
         keep, other = call(
             attend_kernel,
             [((tokens, width), BF16)] * 2,
@@ -775,9 +755,9 @@
                 pos,
                 mine,
                 theirs,
-                attend_prenormal_scale.reshape(1, embed),
+                before,
                 shift,
-                unit.reshape(1, val_w),
+                unit,
                 spike_o,
                 from_x,
                 from_y,
@@ -797,7 +777,7 @@
                 pltpu.VMEM((tokens, LANES), BF16),
                 pltpu.SemaphoreType.DMA((48,)),
             ],
-            grant=56,
+            fixed=True,
             flops=10**10,
             free=7,
         )
@@ -810,19 +790,16 @@
         (hidden,) = call(
             expand_kernel,
             [((tokens, ff), BF16)],
-            (pos, mine, theirs, perceptron_scale.reshape(1, embed), taps_v, taps_g) + up,
+            (pos, mine, theirs, after, taps_v, taps_g) + up,
             scratch=[pltpu.VMEM((embed, 2 * ff), BF16), pltpu.SemaphoreType.DMA((8,))],
             flops=10**10,
             free=14,
         )
         half = width // 2
         parts = []
-        for kernel, places in (
-            (contract_kernel_one, (0, 3, 4)), (contract_kernel_two, (1, 2, 5, 6))
-        ):
-            slots = tuple(group[place] for group in (down_own, down_across) for place in places)
+        for slots in (down_own, down_across):
             keep, other = call(
-                kernel,
+                contract_kernel,
                 [((tokens, half), BF16)] * 2,
                 (pos, hidden) + slots,
                 scratch=[
@@ -830,16 +807,17 @@
                     pltpu.SemaphoreType.DMA((4,)),
                 ],
                 flops=10**10,
-                free=len(slots),
+                free=7,
             )
             pieces = reduce(keep, move(other, over_c))
             total = pieces[0].astype(F32)
             for piece in pieces[1:]:
                 total = total + piece.astype(F32)
             parts.append(total.astype(BF16).astype(F32))
-        even = lax.rem(z, 2) == 0
+        shard = half // 2
+        first, second = parts
         ffn = jnp.concatenate(
-            [jnp.where(even, parts[0], parts[1]), jnp.where(even, parts[1], parts[0])], axis=1
+            [first[:, :shard], second[:, :shard], first[:, shard:], second[:, shard:]], axis=1
         )
         return (middle.astype(F32) + ffn).astype(BF16)
 

time: 265 us -> 279 us (1.053)
  starting transfers between devices: 69 us -> 75.5 us
  local copies, waits for them, and re-layouts: 5.55 us -> 11.6 us
  waiting for transfers between devices: 149 us -> 153 us
  Pallas kernels: 32.5 us -> 29.5 us
    ppermute x53, starting transfers between devices: 69 us -> 75.5 us  [move(): return lax.ppermute(value, axes, perm)]
    ppermute x53, waiting for transfers between devices: 149 us -> 153 us  [move(): return lax.ppermute(value, axes, perm)]
    unnamed x37 -> x23, local copies, waits for them, and re-layouts: 1.71 us -> 4.79 us
    pallas_call x6, Pallas kernels: 32.5 us -> 29.5 us  [call(): pl.pallas_call(kernel, out_shape=[jax.ShapeDtypeStruct(*o) for o in outs]...]
  transfers between devices with their start and end apart: 53 -> 53, of which waited for: 24 -> 23; matrix products, arithmetic and copies ran while one was open for 2% -> 4% of each run, Pallas kernels for 5% -> 5%
where the time goes in v2:
time: 279 us; the launch traced here: 278 us
  waiting for transfers between devices  153 us (55%)
  starting transfers between devices  75.5 us (27%)
  Pallas kernels  29.5 us (11%)
  local copies, waits for them, and re-layouts  11.6 us (4%)
  other arithmetic  7.89 us (3%)
    ppermute x53, waiting for transfers between devices, move(): return lax.ppermute(value, axes, perm)  153 us
    ppermute x53, starting transfers between devices, move(): return lax.ppermute(value, axes, perm)  75.5 us
    pallas_call x6, Pallas kernels, call(): pl.pallas_call(kernel, out_shape=[jax.ShapeDtypeStruct(*o) for o in outs]...  29.5 us
  transfers between devices with their start and end apart: 53, of which 23 were waited for; matrix products, arithmetic and copies ran while one was open for 4% of the time, Pallas kernels for 5%

profile of v2, /device:TPU:0, one launch (start us, length us, event | category | flops | bytes accessed | tf_op | source)
XLA Modules:
  0.0 278.1 jit_solution(1492065395299723111)
XLA Ops:
  0.6 2.3 shard_map.164
  3.0 3.0 %collective-permute-start.4 = (bf16[1152,128]{1,0:T(8,128)(2,1)}, bf16[1152,128]{1,0:T(8,128)(2,1)S(1)}, u32[]{:S(2)}, u32[]{:S(2)}) collective-permute-start(bf16[1152,128]{1,0:T(8,128)(2,1)} %get-tuple-element.22), channel_id=1, source_target_pairs={{0,2},{1,3},{2,0},{3,1},{4,6},{5,7},{6,4},{7,5},{8,10},{9,11},{10,... | collective-permute-start | bytes 884744 | tf_op jit(solution)/shard_map/ppermute | solution.py:622
  6.0 2.8 %shard_map.163 = (bf16[192,128]{1,0:T(8,128)(2,1)}, bf16[192,1152]{1,0:T(8,128)(2,1)}, bf16[192,1152]{1,0:T(8,128)(2,1)}, bf16[192,1152]{1,0:T(8,128)(2,1)}) custom-call(s32[9]{0:T(128)} %stack.32.pos, f32[192,256]{1,0:T(8,128)} %spike.1, bf16[192,1024]{1,0:T(8,128)(2,1)} %feat.1), custom_call_target="tpu_custom_call" | custom-call | bytes 1048576 | tf_op jit(solution)/shard_map/pallas_call | solution.py:579
  15.3 4.6 %collective-permute-start.5 = (bf16[2304,128]{1,0:T(8,128)(2,1)S(1)}, bf16[2304,128]{1,0:T(8,128)(2,1)S(1)}, u32[]{:S(2)}, u32[]{:S(2)}) collective-permute-start(bf16[2304,128]{1,0:T(8,128)(2,1)S(1)} %constant_dynamic-update-slice_fusion.slot_o), channel_id=1, source_target_pairs={{0,4},{1,5},{2,6},{3,7},{4,8},{5,9},{6,10},{7,11},{8,12},{9,13},{1... | collective-permute-start | bytes 1769480 | tf_op jit(solution)/shard_map/ppermute | solution.py:622
  19.9 2.1 collective-permute-done.spike_x
  22.1 10.0 %collective-permute-done.1.spike_y = bf16[192,1152]{1,0:T(8,128)(2,1)S(1)} collective-permute-done((bf16[192,1152]{1,0:T(8,128)(2,1)}, bf16[192,1152]{1,0:T(8,128)(2,1)S(1)}, u32[]{:S(2)}, u32[]{:S(2)}) %collective-permute-start.1) | collective-permute-done | bytes 442400 | tf_op jit(solution)/shard_map/ppermute | solution.py:622
  36.9 13.3 %collective-permute-done.8.slot_l2 = bf16[2304,128]{1,0:T(8,128)(2,1)} collective-permute-done((bf16[2304,128]{1,0:T(8,128)(2,1)S(1)}, bf16[2304,128]{1,0:T(8,128)(2,1)}, u32[]{:S(2)}, u32[]{:S(2)}) %collective-permute-start.8) | collective-permute-done | bytes 589856 | tf_op jit(solution)/shard_map/ppermute | solution.py:622
  55.9 11.5 %collective-permute-done.10.slot_l3 = bf16[2304,128]{1,0:T(8,128)(2,1)} collective-permute-done((bf16[2304,128]{1,0:T(8,128)(2,1)}, bf16[2304,128]{1,0:T(8,128)(2,1)}, u32[]{:S(2)}, u32[]{:S(2)}) %collective-permute-start.10) | collective-permute-done | bytes 589856 | tf_op jit(solution)/shard_map/ppermute | solution.py:622
  69.5 13.9 %shard_map.165 = (bf16[768,1024]{1,0:T(8,128)(2,1)S(1)}, bf16[768,1024]{1,0:T(8,128)(2,1)S(1)}) custom-call(s32[9]{0:T(128)S(1)} %copy-done.1, bf16[768,1024]{1,0:T(8,128)(2,1)S(1)} %pad_maximum_fusion.mine, bf16[768,1024]{1,0:T(8,128)(2,1)} %collective-permute-done.3.theirs, bf16[1,2048]{1,0:T(2,128)(2,1)S(1)} %reshape.12.scale, ...), custom_call_target="tpu_custom_call" | custom-call | flops 10000000000 | bytes 1048576 | tf_op jit(solution)/shard_map/pallas_call | solution.py:579
  83.5 3.4 %collective-permute-done.11 = bf16[768,1024]{1,0:T(8,128)(2,1)S(1)} collective-permute-done((bf16[768,1024]{1,0:T(8,128)(2,1)S(1)}, bf16[768,1024]{1,0:T(8,128)(2,1)S(1)}, u32[]{:S(2)}, u32[]{:S(2)}) %collective-permute-start.11) | collective-permute-done | bytes 1572896 | tf_op jit(solution)/shard_map/ppermute | solution.py:622
  94.2 1.6 collective-permute-start.25
  97.3 3.7 %collective-permute-done.12 = bf16[192,1024]{1,0:T(8,128)(2,1)} collective-permute-done((bf16[192,1024]{1,0:T(8,128)(2,1)}, bf16[192,1024]{1,0:T(8,128)(2,1)}, u32[]{:S(2)}, u32[]{:S(2)}) %collective-permute-start.12) | collective-permute-done | bytes 393248 | tf_op jit(solution)/shard_map/ppermute | solution.py:622
  100.9 10.0 %collective-permute-done.13 = bf16[192,1024]{1,0:T(8,128)(2,1)} collective-permute-done((bf16[192,1024]{1,0:T(8,128)(2,1)}, bf16[192,1024]{1,0:T(8,128)(2,1)}, u32[]{:S(2)}, u32[]{:S(2)}) %collective-permute-start.13) | collective-permute-done | bytes 393248 | tf_op jit(solution)/shard_map/ppermute | solution.py:622
  113.1 1.6 collective-permute-start.16
  116.2 20.1 %collective-permute-done.32 = bf16[512,256]{1,0:T(8,128)(2,1)} collective-permute-done((bf16[512,256]{1,0:T(8,128)(2,1)S(1)}, bf16[512,256]{1,0:T(8,128)(2,1)}, u32[]{:S(2)}, u32[]{:S(2)}) %collective-permute-start.32) | collective-permute-done | bytes 262176 | tf_op jit(solution)/shard_map/ppermute | solution.py:622
  140.0 7.7 %collective-permute-start.33 = (bf16[512,256]{1,0:T(8,128)(2,1)S(1)}, bf16[512,256]{1,0:T(8,128)(2,1)S(1)}, u32[]{:S(2)}, u32[]{:S(2)}) collective-permute-start(bf16[512,256]{1,0:T(8,128)(2,1)S(1)} %get-tuple-element.32.slot_o), channel_id=1, source_target_pairs={{0,4},{1,5},{2,6},{3,7},{4,8},{5,9},{6,10},{7,11},{8,12},{9,13},{1... | collective-permute-start | bytes 786440 | tf_op jit(solution)/shard_map/ppermute | solution.py:622
  147.7 4.7 %collective-permute-start.26 = (bf16[256,1024]{1,0:T(8,128)(2,1)S(1)}, bf16[256,1024]{1,0:T(8,128)(2,1)S(1)}, u32[]{:S(2)}, u32[]{:S(2)}) collective-permute-start(bf16[256,1024]{1,0:T(8,128)(2,1)S(1)} %collective-permute-done.25.refs_7_), channel_id=1, source_target_pairs={{0,4},{1,5},{2,6},{3,7},{4,8},{5,9},{6,10},{7,11},{8,12},{9,13},{1... | collective-permute-start | bytes 1572872 | tf_op jit(solution)/shard_map/ppermute | solution.py:622
  156.3 6.1 %collective-permute-start.43 = (bf16[512,256]{1,0:T(8,128)(2,1)S(1)}, bf16[512,256]{1,0:T(8,128)(2,1)S(1)}, u32[]{:S(2)}, u32[]{:S(2)}) collective-permute-start(bf16[512,256]{1,0:T(8,128)(2,1)S(1)} %get-tuple-element.33.slot_o), channel_id=1, source_target_pairs={{0,4},{1,5},{2,6},{3,7},{4,8},{5,9},{6,10},{7,11},{8,12},{9,13},{1... | collective-permute-start | bytes 786440 | tf_op jit(solution)/shard_map/ppermute | solution.py:622
  162.5 8.6 %collective-permute-done.34.slot_l1 = bf16[512,256]{1,0:T(8,128)(2,1)S(1)} collective-permute-done((bf16[512,256]{1,0:T(8,128)(2,1)S(1)}, bf16[512,256]{1,0:T(8,128)(2,1)S(1)}, u32[]{:S(2)}, u32[]{:S(2)}) %collective-permute-start.34) | collective-permute-done | bytes 262176 | tf_op jit(solution)/shard_map/ppermute | solution.py:622
  175.8 16.4 %collective-permute-done.22.refs_4_ = bf16[256,1024]{1,0:T(8,128)(2,1)S(1)} collective-permute-done((bf16[256,1024]{1,0:T(8,128)(2,1)S(1)}, bf16[256,1024]{1,0:T(8,128)(2,1)S(1)}, u32[]{:S(2)}, u32[]{:S(2)}) %collective-permute-start.22) | collective-permute-done | bytes 524320 | tf_op jit(solution)/shard_map/ppermute | solution.py:622
  194.3 9.2 %collective-permute-done.29.refs_11_ = bf16[256,1024]{1,0:T(8,128)(2,1)S(1)} collective-permute-done((bf16[256,1024]{1,0:T(8,128)(2,1)S(1)}, bf16[256,1024]{1,0:T(8,128)(2,1)S(1)}, u32[]{:S(2)}, u32[]{:S(2)}) %collective-permute-start.29) | collective-permute-done | bytes 524320 | tf_op jit(solution)/shard_map/ppermute | solution.py:622
  207.0 7.7 %collective-permute-done.24.refs_6_ = bf16[256,1024]{1,0:T(8,128)(2,1)S(1)} collective-permute-done((bf16[256,1024]{1,0:T(8,128)(2,1)S(1)}, bf16[256,1024]{1,0:T(8,128)(2,1)S(1)}, u32[]{:S(2)}, u32[]{:S(2)}) %collective-permute-start.24) | collective-permute-done | bytes 524320 | tf_op jit(solution)/shard_map/ppermute | solution.py:622
  216.1 9.0 %collective-permute-done.31.refs_13_ = bf16[256,1024]{1,0:T(8,128)(2,1)S(1)} collective-permute-done((bf16[256,1024]{1,0:T(8,128)(2,1)S(1)}, bf16[256,1024]{1,0:T(8,128)(2,1)S(1)}, u32[]{:S(2)}, u32[]{:S(2)}) %collective-permute-start.31) | collective-permute-done | bytes 524320 | tf_op jit(solution)/shard_map/ppermute | solution.py:622
  227.7 7.0 %shard_map.166.hidden = bf16[768,512]{1,0:T(8,128)(2,1)S(1)} custom-call(s32[9]{0:T(128)S(1)} %copy-done.1, bf16[768,1024]{1,0:T(8,128)(2,1)S(1)} %pad_maximum_fusion.1.mine, bf16[768,1024]{1,0:T(8,128)(2,1)S(1)} %collective-permute-done.18.theirs, bf16[1,2048]{1,0:T(2,128)(2,1)S(1)} %reshape.15.scale, bf16[3,512]{1,0:T(4,128)(2,1)S(1)} %get-tuple-element.51.taps_v, ...), custom_call_target="tpu_custom_call" | custom-call | flops 10000000000 | bytes 1048576 | tf_op jit(solution)/shard_map/pallas_call | solution.py:579
  239.2 1.7 shard_map.167
  241.0 10.3 %collective-permute-done.46.slot_l2 = bf16[512,256]{1,0:T(8,128)(2,1)S(1)} collective-permute-done((bf16[512,256]{1,0:T(8,128)(2,1)S(1)}, bf16[512,256]{1,0:T(8,128)(2,1)S(1)}, u32[]{:S(2)}, u32[]{:S(2)}) %collective-permute-start.46) | collective-permute-done | bytes 262176 | tf_op jit(solution)/shard_map/ppermute | solution.py:622
  251.2 2.8 %collective-permute-done.48.slot_l3 = bf16[512,256]{1,0:T(8,128)(2,1)S(1)} collective-permute-done((bf16[512,256]{1,0:T(8,128)(2,1)S(1)}, bf16[512,256]{1,0:T(8,128)(2,1)S(1)}, u32[]{:S(2)}, u32[]{:S(2)}) %collective-permute-start.48) | collective-permute-done | bytes 262176 | tf_op jit(solution)/shard_map/ppermute | solution.py:622
  254.1 1.7 shard_map.168
  262.0 1.9 collective-permute-done.40
  265.4 2.2 collective-permute-done.41
  269.3 3.1 %collective-permute-done.50 = bf16[192,512]{1,0:T(8,128)(2,1)S(1)} collective-permute-done((bf16[192,512]{1,0:T(8,128)(2,1)S(1)}, bf16[192,512]{1,0:T(8,128)(2,1)S(1)}, u32[]{:S(2)}, u32[]{:S(2)}) %collective-permute-start.50) | collective-permute-done | bytes 196640 | tf_op jit(solution)/shard_map/ppermute | solution.py:622
  272.4 4.7 %collective-permute-done.52 = bf16[192,512]{1,0:T(8,128)(2,1)S(1)} collective-permute-done((bf16[192,512]{1,0:T(8,128)(2,1)S(1)}, bf16[192,512]{1,0:T(8,128)(2,1)S(1)}, u32[]{:S(2)}, u32[]{:S(2)}) %collective-permute-start.52) | collective-permute-done | bytes 196640 | tf_op jit(solution)/shard_map/ppermute | solution.py:622
  (133 shorter events, 68.4 us)
Async XLA Ops:
  10.3 21.8 %collective-permute-start.1 = (bf16[192,1152]{1,0:T(8,128)(2,1)}, bf16[192,1152]{1,0:T(8,128)(2,1)S(1)}, u32[]{:S(2)}, u32[]{:S(2)}) collective-permute-start(bf16[192,1152]{1,0:T(8,128)(2,1)} %get-tuple-element.18), channel_id=1, source_target_pairs={{0,2},{1,3},{2,0},{3,1},{4,6},{5,7},{6,4},{7,5},{8,10},{9,11},{10,... | collective-permute-start | bytes 1327112 | tf_op jit(solution)/shard_map/ppermute | solution.py:622
  10.8 21.4 %collective-permute-start.2 = (bf16[192,1152]{1,0:T(8,128)(2,1)}, bf16[192,1152]{1,0:T(8,128)(2,1)S(1)}, u32[]{:S(2)}, u32[]{:S(2)}) collective-permute-start(bf16[192,1152]{1,0:T(8,128)(2,1)} %get-tuple-element.19), channel_id=1, source_target_pairs={{0,18},{1,19},{2,16},{3,17},{4,22},{5,23},{6,20},{7,21},{8,26},{9,... | collective-permute-start | bytes 1327112 | tf_op jit(solution)/shard_map/ppermute | solution.py:622
  14.0 18.5 %collective-permute-start.6 = (bf16[2304,128]{1,0:T(8,128)(2,1)S(1)}, bf16[2304,128]{1,0:T(8,128)(2,1)S(1)}, u32[]{:S(2)}, u32[]{:S(2)}) collective-permute-start(bf16[2304,128]{1,0:T(8,128)(2,1)S(1)} %constant_dynamic-update-slice_fusion.slot_o), channel_id=1, source_target_pairs={{4,0},{5,1},{6,2},{7,3},{8,4},{9,5},{10,6},{11,7},{12,8},{13,9},{1... | collective-permute-start | bytes 1769480 | tf_op jit(solution)/shard_map/ppermute | solution.py:622
  15.3 19.3 %collective-permute-start.5 = (bf16[2304,128]{1,0:T(8,128)(2,1)S(1)}, bf16[2304,128]{1,0:T(8,128)(2,1)S(1)}, u32[]{:S(2)}, u32[]{:S(2)}) collective-permute-start(bf16[2304,128]{1,0:T(8,128)(2,1)S(1)} %constant_dynamic-update-slice_fusion.slot_o), channel_id=1, source_target_pairs={{0,4},{1,5},{2,6},{3,7},{4,8},{5,9},{6,10},{7,11},{8,12},{9,13},{1... | collective-permute-start | bytes 1769480 | tf_op jit(solution)/shard_map/ppermute | solution.py:622
  32.4 23.5 %collective-permute-start.3 = (bf16[768,1024]{1,0:T(8,128)(2,1)S(1)}, bf16[768,1024]{1,0:T(8,128)(2,1)}, u32[]{:S(2)}, u32[]{:S(2)}) collective-permute-start(bf16[768,1024]{1,0:T(8,128)(2,1)S(1)} %pad_maximum_fusion.mine), channel_id=1, source_target_pairs={{0,1},{1,0},{2,3},{3,2},{4,5},{5,4},{6,7},{7,6},{8,9},{9,8},{10,11... | collective-permute-start | bytes 4718600 | tf_op jit(solution)/shard_map/ppermute | solution.py:622
  32.5 17.8 %collective-permute-start.8 = (bf16[2304,128]{1,0:T(8,128)(2,1)S(1)}, bf16[2304,128]{1,0:T(8,128)(2,1)}, u32[]{:S(2)}, u32[]{:S(2)}) collective-permute-start(bf16[2304,128]{1,0:T(8,128)(2,1)S(1)} %collective-permute-done.6.slot_l1), channel_id=1, source_target_pairs={{4,0},{5,1},{6,2},{7,3},{8,4},{9,5},{10,6},{11,7},{20,16},{21,17},... | collective-permute-start | bytes 1769480 | tf_op jit(solution)/shard_map/ppermute | solution.py:622
  34.6 16.9 %collective-permute-start.7 = (bf16[2304,128]{1,0:T(8,128)(2,1)S(1)}, bf16[2304,128]{1,0:T(8,128)(2,1)}, u32[]{:S(2)}, u32[]{:S(2)}) collective-permute-start(bf16[2304,128]{1,0:T(8,128)(2,1)S(1)} %collective-permute-done.5.slot_r1), channel_id=1, source_target_pairs={{4,8},{5,9},{6,10},{7,11},{8,12},{9,13},{10,14},{11,15},{20,24},{2... | collective-permute-start | bytes 1769480 | tf_op jit(solution)/shard_map/ppermute | solution.py:622
  50.3 17.1 %collective-permute-start.10 = (bf16[2304,128]{1,0:T(8,128)(2,1)}, bf16[2304,128]{1,0:T(8,128)(2,1)}, u32[]{:S(2)}, u32[]{:S(2)}) collective-permute-start(bf16[2304,128]{1,0:T(8,128)(2,1)} %collective-permute-done.8.slot_l2), channel_id=1, source_target_pairs={{4,0},{5,1},{6,2},{7,3},{20,16},{21,17},{22,18},{23,19}} | collective-permute-start | bytes 1769480 | tf_op jit(solution)/shard_map/ppermute | solution.py:622
  90.2 20.7 %collective-permute-start.13 = (bf16[192,1024]{1,0:T(8,128)(2,1)}, bf16[192,1024]{1,0:T(8,128)(2,1)}, u32[]{:S(2)}, u32[]{:S(2)}) collective-permute-start(bf16[192,1024]{1,0:T(8,128)(2,1)} %get-tuple-element.31), channel_id=1, source_target_pairs={{0,2},{1,3},{2,0},{3,1},{4,6},{5,7},{6,4},{7,5},{8,10},{9,11},{10,... | collective-permute-start | bytes 1179656 | tf_op jit(solution)/shard_map/ppermute | solution.py:622
  91.7 19.2 %collective-permute-start.14 = (bf16[192,1024]{1,0:T(8,128)(2,1)}, bf16[192,1024]{1,0:T(8,128)(2,1)}, u32[]{:S(2)}, u32[]{:S(2)}) collective-permute-start(bf16[192,1024]{1,0:T(8,128)(2,1)} %get-tuple-element.30), channel_id=1, source_target_pairs={{0,18},{1,19},{2,16},{3,17},{4,22},{5,23},{6,20},{7,21},{8,26},{9,... | collective-permute-start | bytes 1179656 | tf_op jit(solution)/shard_map/ppermute | solution.py:622
  94.2 43.4 %collective-permute-start.25 = (bf16[256,1024]{1,0:T(8,128)(2,1)}, bf16[256,1024]{1,0:T(8,128)(2,1)S(1)}, u32[]{:S(2)}, u32[]{:S(2)}) collective-permute-start(bf16[256,1024]{1,0:T(8,128)(2,1)} %pad_maximum_fusion.3), channel_id=1, source_target_pairs={{0,2},{1,3},{2,0},{3,1},{4,6},{5,7},{6,4},{7,5},{8,10},{9,11},{10,... | collective-permute-start | bytes 1572872 | tf_op jit(solution)/shard_map/ppermute | solution.py:622
  96.8 39.5 %collective-permute-start.32 = (bf16[512,256]{1,0:T(8,128)(2,1)S(1)}, bf16[512,256]{1,0:T(8,128)(2,1)}, u32[]{:S(2)}, u32[]{:S(2)}) collective-permute-start(bf16[512,256]{1,0:T(8,128)(2,1)S(1)} %constant_dynamic-slice_fusion), channel_id=1, source_target_pairs={{0,2},{1,3},{2,0},{3,1},{4,6},{5,7},{6,4},{7,5},{8,10},{9,11},{10,... | collective-permute-start | bytes 786440 | tf_op jit(solution)/shard_map/ppermute | solution.py:622
  112.5 27.5 %collective-permute-start.15 = (bf16[192,1024]{1,0:T(8,128)(2,1)S(1)}, bf16[192,1024]{1,0:T(8,128)(2,1)S(1)}, u32[]{:S(2)}, u32[]{:S(2)}) collective-permute-start(bf16[192,1024]{1,0:T(8,128)(2,1)S(1)} %add_convert_fusion.3), channel_id=1, source_target_pairs={{0,16},{1,17},{2,18},{3,19},{4,20},{5,21},{6,22},{7,23},{8,24},{9,... | collective-permute-start | bytes 1179656 | tf_op jit(solution)/shard_map/ppermute | solution.py:622
  113.1 34.6 %collective-permute-start.16 = (bf16[192,1024]{1,0:T(8,128)(2,1)S(1)}, bf16[192,1024]{1,0:T(8,128)(2,1)S(1)}, u32[]{:S(2)}, u32[]{:S(2)}) collective-permute-start(bf16[192,1024]{1,0:T(8,128)(2,1)S(1)} %add_convert_fusion.3), channel_id=1, source_target_pairs={{0,2},{1,3},{2,0},{3,1},{4,6},{5,7},{6,4},{7,5},{8,10},{9,11},{10,... | collective-permute-start | bytes 1179656 | tf_op jit(solution)/shard_map/ppermute | solution.py:622
  114.7 37.8 %collective-permute-start.17 = (bf16[192,1024]{1,0:T(8,128)(2,1)S(1)}, bf16[192,1024]{1,0:T(8,128)(2,1)}, u32[]{:S(2)}, u32[]{:S(2)}) collective-permute-start(bf16[192,1024]{1,0:T(8,128)(2,1)S(1)} %add_convert_fusion.3), channel_id=1, source_target_pairs={{0,18},{1,19},{2,16},{3,17},{4,22},{5,23},{6,20},{7,21},{8,26},{9,... | collective-permute-start | bytes 1179656 | tf_op jit(solution)/shard_map/ppermute | solution.py:622
  136.2 18.7 %collective-permute-start.19 = (bf16[256,1024]{1,0:T(8,128)(2,1)S(1)}, bf16[256,1024]{1,0:T(8,128)(2,1)S(1)}, u32[]{:S(2)}, u32[]{:S(2)}) collective-permute-start(bf16[256,1024]{1,0:T(8,128)(2,1)S(1)} %pad_maximum_fusion.2.refs_0_), channel_id=1, source_target_pairs={{0,4},{1,5},{2,6},{3,7},{4,8},{5,9},{6,10},{7,11},{8,12},{9,13},{1... | collective-permute-start | bytes 1572872 | tf_op jit(solution)/shard_map/ppermute | solution.py:622
  137.6 17.5 %collective-permute-start.20 = (bf16[256,1024]{1,0:T(8,128)(2,1)S(1)}, bf16[256,1024]{1,0:T(8,128)(2,1)S(1)}, u32[]{:S(2)}, u32[]{:S(2)}) collective-permute-start(bf16[256,1024]{1,0:T(8,128)(2,1)S(1)} %pad_maximum_fusion.2.refs_0_), channel_id=1, source_target_pairs={{4,0},{5,1},{6,2},{7,3},{8,4},{9,5},{10,6},{11,7},{12,8},{13,9},{1... | collective-permute-start | bytes 1572872 | tf_op jit(solution)/shard_map/ppermute | solution.py:622
  140.0 16.3 %collective-permute-start.33 = (bf16[512,256]{1,0:T(8,128)(2,1)S(1)}, bf16[512,256]{1,0:T(8,128)(2,1)S(1)}, u32[]{:S(2)}, u32[]{:S(2)}) collective-permute-start(bf16[512,256]{1,0:T(8,128)(2,1)S(1)} %get-tuple-element.32.slot_o), channel_id=1, source_target_pairs={{0,4},{1,5},{2,6},{3,7},{4,8},{5,9},{6,10},{7,11},{8,12},{9,13},{1... | collective-permute-start | bytes 786440 | tf_op jit(solution)/shard_map/ppermute | solution.py:622
  147.7 25.4 %collective-permute-start.26 = (bf16[256,1024]{1,0:T(8,128)(2,1)S(1)}, bf16[256,1024]{1,0:T(8,128)(2,1)S(1)}, u32[]{:S(2)}, u32[]{:S(2)}) collective-permute-start(bf16[256,1024]{1,0:T(8,128)(2,1)S(1)} %collective-permute-done.25.refs_7_), channel_id=1, source_target_pairs={{0,4},{1,5},{2,6},{3,7},{4,8},{5,9},{6,10},{7,11},{8,12},{9,13},{1... | collective-permute-start | bytes 1572872 | tf_op jit(solution)/shard_map/ppermute | solution.py:622
  152.5 21.4 %collective-permute-start.27 = (bf16[256,1024]{1,0:T(8,128)(2,1)S(1)}, bf16[256,1024]{1,0:T(8,128)(2,1)S(1)}, u32[]{:S(2)}, u32[]{:S(2)}) collective-permute-start(bf16[256,1024]{1,0:T(8,128)(2,1)S(1)} %collective-permute-done.25.refs_7_), channel_id=1, source_target_pairs={{4,0},{5,1},{6,2},{7,3},{8,4},{9,5},{10,6},{11,7},{12,8},{13,9},{1... | collective-permute-start | bytes 1572872 | tf_op jit(solution)/shard_map/ppermute | solution.py:622
  154.9 71.5 %collective-permute-start.18 = (bf16[768,1024]{1,0:T(8,128)(2,1)S(1)}, bf16[768,1024]{1,0:T(8,128)(2,1)S(1)}, u32[]{:S(2)}, u32[]{:S(2)}) collective-permute-start(bf16[768,1024]{1,0:T(8,128)(2,1)S(1)} %pad_maximum_fusion.1.mine), channel_id=1, source_target_pairs={{0,1},{1,0},{2,3},{3,2},{4,5},{5,4},{6,7},{7,6},{8,9},{9,8},{10,11... | collective-permute-start | bytes 4718600 | tf_op jit(solution)/shard_map/ppermute | solution.py:622
  171.8 20.5 %collective-permute-start.22 = (bf16[256,1024]{1,0:T(8,128)(2,1)S(1)}, bf16[256,1024]{1,0:T(8,128)(2,1)S(1)}, u32[]{:S(2)}, u32[]{:S(2)}) collective-permute-start(bf16[256,1024]{1,0:T(8,128)(2,1)S(1)} %collective-permute-done.20.refs_2_), channel_id=1, source_target_pairs={{4,0},{5,1},{6,2},{7,3},{8,4},{9,5},{10,6},{11,7},{20,16},{21,17},... | collective-permute-start | bytes 1572872 | tf_op jit(solution)/shard_map/ppermute | solution.py:622
  173.1 20.4 %collective-permute-start.28 = (bf16[256,1024]{1,0:T(8,128)(2,1)S(1)}, bf16[256,1024]{1,0:T(8,128)(2,1)S(1)}, u32[]{:S(2)}, u32[]{:S(2)}) collective-permute-start(bf16[256,1024]{1,0:T(8,128)(2,1)S(1)} %collective-permute-done.26.refs_8_), channel_id=1, source_target_pairs={{4,8},{5,9},{6,10},{7,11},{8,12},{9,13},{10,14},{11,15},{20,24},{2... | collective-permute-start | bytes 1572872 | tf_op jit(solution)/shard_map/ppermute | solution.py:622
  173.8 29.7 %collective-permute-start.29 = (bf16[256,1024]{1,0:T(8,128)(2,1)S(1)}, bf16[256,1024]{1,0:T(8,128)(2,1)S(1)}, u32[]{:S(2)}, u32[]{:S(2)}) collective-permute-start(bf16[256,1024]{1,0:T(8,128)(2,1)S(1)} %collective-permute-done.27.refs_9_), channel_id=1, source_target_pairs={{4,0},{5,1},{6,2},{7,3},{8,4},{9,5},{10,6},{11,7},{20,16},{21,17},... | collective-permute-start | bytes 1572872 | tf_op jit(solution)/shard_map/ppermute | solution.py:622
  175.1 30.4 %collective-permute-start.23 = (bf16[256,1024]{1,0:T(8,128)(2,1)S(1)}, bf16[256,1024]{1,0:T(8,128)(2,1)S(1)}, u32[]{:S(2)}, u32[]{:S(2)}) collective-permute-start(bf16[256,1024]{1,0:T(8,128)(2,1)S(1)} %collective-permute-done.21.refs_3_), channel_id=1, source_target_pairs={{8,12},{9,13},{10,14},{11,15},{24,28},{25,29},{26,30},{27,31}} | collective-permute-start | bytes 1572872 | tf_op jit(solution)/shard_map/ppermute | solution.py:622
  192.3 22.5 %collective-permute-start.24 = (bf16[256,1024]{1,0:T(8,128)(2,1)S(1)}, bf16[256,1024]{1,0:T(8,128)(2,1)S(1)}, u32[]{:S(2)}, u32[]{:S(2)}) collective-permute-start(bf16[256,1024]{1,0:T(8,128)(2,1)S(1)} %collective-permute-done.22.refs_4_), channel_id=1, source_target_pairs={{4,0},{5,1},{6,2},{7,3},{20,16},{21,17},{22,18},{23,19}} | collective-permute-start | bytes 1572872 | tf_op jit(solution)/shard_map/ppermute | solution.py:622
  193.6 21.8 %collective-permute-start.30 = (bf16[256,1024]{1,0:T(8,128)(2,1)S(1)}, bf16[256,1024]{1,0:T(8,128)(2,1)S(1)}, u32[]{:S(2)}, u32[]{:S(2)}) collective-permute-start(bf16[256,1024]{1,0:T(8,128)(2,1)S(1)} %collective-permute-done.28.refs_10_), channel_id=1, source_target_pairs={{8,12},{9,13},{10,14},{11,15},{24,28},{25,29},{26,30},{27,31}} | collective-permute-start | bytes 1572872 | tf_op jit(solution)/shard_map/ppermute | solution.py:622
  203.5 21.6 %collective-permute-start.31 = (bf16[256,1024]{1,0:T(8,128)(2,1)S(1)}, bf16[256,1024]{1,0:T(8,128)(2,1)S(1)}, u32[]{:S(2)}, u32[]{:S(2)}) collective-permute-start(bf16[256,1024]{1,0:T(8,128)(2,1)S(1)} %collective-permute-done.29.refs_11_), channel_id=1, source_target_pairs={{4,0},{5,1},{6,2},{7,3},{20,16},{21,17},{22,18},{23,19}} | collective-permute-start | bytes 1572872 | tf_op jit(solution)/shard_map/ppermute | solution.py:622
  205.6 29.2 %collective-permute-start.44 = (bf16[512,256]{1,0:T(8,128)(2,1)S(1)}, bf16[512,256]{1,0:T(8,128)(2,1)S(1)}, u32[]{:S(2)}, u32[]{:S(2)}) collective-permute-start(bf16[512,256]{1,0:T(8,128)(2,1)S(1)} %get-tuple-element.33.slot_o), channel_id=1, source_target_pairs={{4,0},{5,1},{6,2},{7,3},{8,4},{9,5},{10,6},{11,7},{12,8},{13,9},{1... | collective-permute-start | bytes 786440 | tf_op jit(solution)/shard_map/ppermute | solution.py:622
  214.8 20.7 %collective-permute-start.35 = (bf16[512,256]{1,0:T(8,128)(2,1)S(1)}, bf16[512,256]{1,0:T(8,128)(2,1)S(1)}, u32[]{:S(2)}, u32[]{:S(2)}) collective-permute-start(bf16[512,256]{1,0:T(8,128)(2,1)S(1)} %collective-permute-done.33.slot_r1), channel_id=1, source_target_pairs={{4,8},{5,9},{6,10},{7,11},{8,12},{9,13},{10,14},{11,15},{20,24},{2... | collective-permute-start | bytes 786440 | tf_op jit(solution)/shard_map/ppermute | solution.py:622
  215.4 22.2 %collective-permute-start.37 = (bf16[512,256]{1,0:T(8,128)(2,1)S(1)}, bf16[512,256]{1,0:T(8,128)(2,1)S(1)}, u32[]{:S(2)}, u32[]{:S(2)}) collective-permute-start(bf16[512,256]{1,0:T(8,128)(2,1)S(1)} %collective-permute-done.33.slot_r1), channel_id=1, source_target_pairs={{4,12},{5,13},{6,14},{7,15},{20,28},{21,29},{22,30},{23,31}} | collective-permute-start | bytes 786440 | tf_op jit(solution)/shard_map/ppermute | solution.py:622
  237.7 16.4 %collective-permute-start.48 = (bf16[512,256]{1,0:T(8,128)(2,1)S(1)}, bf16[512,256]{1,0:T(8,128)(2,1)S(1)}, u32[]{:S(2)}, u32[]{:S(2)}) collective-permute-start(bf16[512,256]{1,0:T(8,128)(2,1)S(1)} %collective-permute-done.44.slot_l1), channel_id=1, source_target_pairs={{8,0},{9,1},{10,2},{11,3},{24,16},{25,17},{26,18},{27,19}} | collective-permute-start | bytes 786440 | tf_op jit(solution)/shard_map/ppermute | solution.py:622
  (32 other events, 475.3 us)
